TPU v7x, 32 devices: a whole 2x2x4 slice. The times are simulated.
32 devices in a mesh: sp: 8 (over z, x), tp: 4 (over y, core).
Axes of the slice: x: 2, y: 2, z: 4, core: 2. Of those that a mesh axis runs over, the one named last changes fastest.
Arguments:
- queries: bfloat16 [6144, 2048], P('sp', 'tp'), may hold values from -110 to 110
- key_rows: bfloat16 [6144, 512], P('sp', 'tp'), may hold values from -4.5 to 4.5
- values: bfloat16 [6144, 512], P('sp', 'tp'), may hold values from -6 to 6
- sink_logits: float32 [32], P('tp'), may hold values from 2 to 7
- doc_ids: int32 [6144], P('sp'), may hold values from 0 to 3, as said below
- residual: bfloat16 [6144, 2048], P('sp'), may hold values from -20 to 20
- w_out: bfloat16 [2048, 2048], P('tp'), may hold values from -2.390625 to 2.390625
- norm_gain: float32 [2048], replicated, may hold values from 0.1 to 1.9
- w_value_up: bfloat16 [2048, 5632], P('sp', 'tp'), may hold values from -0.125 to 0.125
- w_gate_up: bfloat16 [2048, 5632], P('sp', 'tp'), may hold values from -0.125 to 0.125
- conv_taps: bfloat16 [3, 5632], P(None, 'tp'), may hold values from -3.5 to 3.5
- w_down_t: bfloat16 [2048, 5632], P('sp', 'tp'), may hold values from -0.078125 to 0.078125
Outputs:
- layer_out: bfloat16 [6144, 2048], P('sp', 'tp')
Inputs may be any that keep to these rules, and one draw needn't show every extreme that they name: `doc_ids`: document numbers never fall along the sequence and every one of the 4 documents is present; each document has 2 or more positions.
All inputs are finite; a program needn't handle non-finite values.
Results may differ from a plain program's by a relative error of at most 0.017.
Values may be sent and summed in bfloat16 or wider, within the bound.
A program may use at most 64 MiB of HBM per device.

v0:
```python
import functools

import jax
import jax.numpy as jnp
from jax import lax
from jax.experimental import pallas as pl
from jax.experimental.pallas import tpu as pltpu
from jax.sharding import PartitionSpec as P

HEAD_DIM = 64
WINDOW = 128
EPS = 1e-06
NEG = -1e30
RIM = 16
MESH = pl.DeviceIdType.MESH
F32 = jnp.float32
BF16 = jnp.bfloat16


def kernel(
    n, ntp,
    q_ref, k_ref, v_ref, sink_ref, lab_row_ref,
    res_hbm, wout_ref, gain_ref, wv_hbm, wg_hbm, taps_ref, wd_hbm,
    out_ref,
    up, down, kx, vx, lx, lc, part, first, second, mixed, normed, value, gate, rim, pd, box, inbox, res,
    loc_sem, ring_send, ring_recv, halo_send, halo_recv, rim_send, rim_recv,
    core_send, core_recv, y_send, y_recv, back_send, back_recv, pair_send, pair_recv,
    down_send, down_recv, out_send, out_recv,
):
    me = lax.axis_index("sp")
    tp = lax.axis_index("tp")
    core = lax.rem(tp, 2)
    y = tp // 2
    ny = ntp // 2
    partner = y * 2 + 1 - core
    rows = q_ref.shape[0]
    half = rows // 2
    piece = half // ny
    block = wv_hbm.shape[0]
    depth = block // 2
    quarter = block // 4

    def place(p):
        h = p // (n // 2)
        return (1 - h) * (2 * p) + h * (2 * n - 1 - 2 * p)

    odd = lax.rem(me, 2)
    pos = (1 - odd) * (me // 2) + odd * ((2 * n - 1 - me) // 2)
    ahead = place(lax.rem(pos + 1, n))
    behind = place(lax.rem(pos + n - 1, n))
    right = lax.rem(me + 1, n)
    left = lax.rem(me + n - 1, n)

    loads = []
    for i, (src, dst) in enumerate((
        (wv_hbm, up.at[0, pl.ds(me * block, block)]),
        (wg_hbm, up.at[1, pl.ds(me * block, block)]),
        (wd_hbm, down.at[pl.ds(me * block, block)]),
        (res_hbm.at[pl.ds(core * half + y * piece, piece)], res),
    )):
        c = pltpu.make_async_copy(src, dst, loc_sem.at[i])
        c.start()
        loads.append(c)

    barrier = pltpu.get_barrier_semaphore()
    peers = [(ahead, tp), (behind, tp), (right, tp), (left, tp)]
    for j in range(1, ntp):
        peers.append((me, lax.rem(tp + j, ntp)))
    for peer in peers:
        pl.semaphore_signal(barrier, inc=1, device_id=peer, device_id_type=MESH)
    for c in loads:
        c.wait()
    pl.semaphore_wait(barrier, len(peers))

    def spot(stream, way, owner):
        if stream < 2:
            return up.at[stream, pl.ds(owner * block + way * depth, depth)]
        return down.at[pl.ds(owner * block + way * depth + (stream - 2) * quarter, quarter)]

    def ring(stream, way, s, arriving):
        shift = s + 1 if arriving else s
        owner = place(lax.rem(pos + n - shift, n)) if way == 0 else place(lax.rem(pos + shift, n))
        ref = spot(stream, way, owner)
        return pltpu.make_async_remote_copy(
            src_ref=ref, dst_ref=ref,
            send_sem=ring_send.at[stream, way, s], recv_sem=ring_recv.at[stream, way, s],
            device_id=(ahead if way == 0 else behind, tp), device_id_type=MESH,
        )

    def begin(stream):
        for way in range(2):
            ring(stream, way, 0, False).start()

    def forward(stream, s, last=False):
        for way in range(2):
            ring(stream, way, s, True).wait_recv()
            if not last:
                ring(stream, way, s + 1, False).start()

    queue = []
    for s in range(n - 1):
        for stream in (0, 1):
            queue.append((stream, s))
    for s in range(n - 1):
        for stream in (2, 3):
            queue.append((stream, s))
    done = [0]

    def serve(count):
        for _ in range(count):
            if done[0] == len(queue):
                return
            stream, s = queue[done[0]]
            done[0] += 1
            forward(stream, s, last=s == n - 2)
            if stream < 2 and s == n - 2:
                begin(stream + 2)

    halo = []

    def remote(src, dst, send, recv, where):
        c = pltpu.make_async_remote_copy(
            src_ref=src, dst_ref=dst, send_sem=send, recv_sem=recv, device_id=where, device_id_type=MESH
        )
        c.start()
        return c

    ends = pl.ds(rows - WINDOW, WINDOW)
    starts = pl.ds(0, WINDOW)
    low, high = pl.ds(0, WINDOW), pl.ds(rows + WINDOW, WINDOW)
    for i, (src, dst) in enumerate(((k_ref, kx), (v_ref, vx))):
        halo.append(remote(src.at[ends], dst.at[low], halo_send.at[i, 0], halo_recv.at[i, 0], (right, tp)))
        halo.append(remote(src.at[starts], dst.at[high], halo_send.at[i, 1], halo_recv.at[i, 1], (left, tp)))
    halo.append(remote(lab_row_ref.at[:, ends], lx.at[:, low], halo_send.at[2, 0], halo_recv.at[2, 0], (right, tp)))
    halo.append(remote(lab_row_ref.at[:, starts], lx.at[:, high], halo_send.at[2, 1], halo_recv.at[2, 1], (left, tp)))
    begin(0)
    begin(1)
    inner = pl.ds(WINDOW, rows)
    kx[inner, :] = k_ref[...]
    vx[inner, :] = v_ref[...]
    lx[:, inner] = lab_row_ref[...]
    for c in halo:
        c.wait()
    lx[:, low] = jnp.where(me == 0, -1, lx[:, low])
    lx[:, high] = jnp.where(me == n - 1, -1, lx[:, high])
    for i in range(rows // WINDOW + 2):
        chunk = slice(i * WINDOW, (i + 1) * WINDOW)
        square = jnp.broadcast_to(lx[0:1, chunk].astype(F32), (WINDOW, WINDOW))
        lc[chunk, :] = jnp.transpose(square)

    kv_local = k_ref.shape[1] // HEAD_DIM
    per_kv = q_ref.shape[1] // k_ref.shape[1]
    blocks = rows // WINDOW
    model = wout_ref.shape[1]

    def attend(b, carry):
        here = pl.ds(pl.multiple_of(b * WINDOW, WINDOW), WINDOW)
        wide = pl.ds(pl.multiple_of(b * WINDOW, WINDOW), 3 * WINDOW)
        q = q_ref[here, :]
        kw = kx[wide, :]
        vw = vx[wide, :]
        lab_k = lx[0:1, wide].astype(F32)
        lab_q = lc[pl.ds(pl.multiple_of(b * WINDOW + WINDOW, WINDOW), WINDOW), 0:1]
        key = lax.broadcasted_iota(jnp.int32, (WINDOW, 3 * WINDOW), 1) - WINDOW
        query = lax.broadcasted_iota(jnp.int32, (WINDOW, 3 * WINDOW), 0)
        allowed = (jnp.abs(key - query) <= WINDOW) & (lab_q == lab_k)
        results = []
        for g in range(kv_local):
            k = kw[:, g * HEAD_DIM:(g + 1) * HEAD_DIM]
            v = vw[:, g * HEAD_DIM:(g + 1) * HEAD_DIM]
            for j in range(per_kv):
                h = g * per_kv + j
                qh = q[:, h * HEAD_DIM:(h + 1) * HEAD_DIM]
                score = lax.dot_general(
                    qh, k, (((1,), (1,)), ((), ())), preferred_element_type=F32
                ) * HEAD_DIM ** (-0.5)
                score = jnp.where(allowed, score, NEG)
                sink = sink_ref[h]
                highest = jnp.maximum(jnp.max(score, axis=1, keepdims=True), sink)
                raw = jnp.where(allowed, jnp.exp(score - highest), 0.0)
                total = jnp.sum(raw, axis=1, keepdims=True) + jnp.exp(sink - highest)
                probs = (raw / total).astype(BF16)
                results.append(jnp.dot(probs, v, preferred_element_type=F32).astype(BF16))
        attended = jnp.concatenate(results, axis=1)
        part[here, :] = jnp.dot(attended, wout_ref[...], preferred_element_type=F32).astype(BF16)
        return carry

    split = blocks // 3
    for t in range(3):
        lax.fori_loop(t * split, (t + 1) * split if t < 2 else blocks, attend, 0)
        serve(2 if t == 1 else 1)

    tile = 32
    other_half = pl.ds((1 - core) * half, half)
    swap = remote(part.at[other_half], first, core_send, core_recv, (me, partner))
    swap.wait()

    def add_first(i, carry):
        r = pl.ds(pl.multiple_of(i * tile, tile), tile)
        o = pl.ds(pl.multiple_of(core * half + i * tile, tile), tile)
        first[r, :] = (part[o, :].astype(F32) + first[r, :].astype(F32)).astype(BF16)
        return carry

    lax.fori_loop(0, half // tile, add_first, 0)
    copies = []
    for j in range(1, ny):
        to = lax.rem(y + j, ny)
        copies.append(remote(
            first.at[pl.ds(to * piece, piece)], second.at[j - 1], y_send.at[j - 1], y_recv.at[j - 1], (me, to * 2 + core)
        ))
    serve(2)
    for c in copies:
        c.wait()

    def add_second(i, carry):
        r = pl.ds(pl.multiple_of(i * tile, tile), tile)
        s = first[pl.ds(pl.multiple_of(y * piece + i * tile, tile), tile), :].astype(F32)
        for j in range(ny - 1):
            s = s + second[j, r, :].astype(F32)
        o = pl.ds(pl.multiple_of(core * half + y * piece + i * tile, tile), tile)
        mixed[o, :] = (res[r, :].astype(F32) + s).astype(BF16)
        return carry

    lax.fori_loop(0, piece // tile, add_second, 0)
    mine = mixed.at[pl.ds(core * half + y * piece, piece)]
    copies = []
    for j in range(1, ny):
        to = lax.rem(y + j, ny)
        copies.append(remote(mine, mine, back_send.at[j - 1], back_recv.at[j - 1], (me, to * 2 + core)))
    serve(2)
    for j, c in enumerate(copies):
        c.wait_send()
        frm = lax.rem(y + ny - (j + 1), ny)
        theirs = mixed.at[pl.ds(core * half + frm * piece, piece)]
        pltpu.make_async_remote_copy(
            src_ref=theirs, dst_ref=theirs, send_sem=back_send.at[j], recv_sem=back_recv.at[j],
            device_id=(me, partner), device_id_type=MESH,
        ).wait_recv()
    own_half = mixed.at[pl.ds(core * half, half)]
    swap = remote(own_half, own_half, pair_send, pair_recv, (me, partner))
    swap.wait_send()
    their_half = mixed.at[other_half]
    pltpu.make_async_remote_copy(
        src_ref=their_half, dst_ref=their_half, send_sem=pair_send, recv_sem=pair_recv,
        device_id=(me, partner), device_id_type=MESH,
    ).wait_recv()

    def normalise(i, carry):
        r = pl.ds(pl.multiple_of(i * tile, tile), tile)
        m = mixed[r, :].astype(F32)
        mean_sq = jnp.mean(m * m, axis=1, keepdims=True)
        normed[r, :] = (m * lax.rsqrt(mean_sq + EPS) * gain_ref[...]).astype(BF16)
        return carry

    lax.fori_loop(0, rows // tile, normalise, 0)

    serve(2 * (n - 1) - done[0])
    big = rows // 3

    def project(t, which, dst):
        r = slice(t * big, (t + 1) * big)
        dst[r, :] = jnp.dot(normed[r, :], up[which], preferred_element_type=F32).astype(BF16)

    for t in range(3):
        project(t, 0, value)
        serve(1)
    tail = remote(value.at[pl.ds(rows - RIM, RIM)], rim.at[0], rim_send.at[0], rim_recv.at[0], (right, tp))
    head = remote(value.at[pl.ds(0, RIM)], rim.at[1], rim_send.at[1], rim_recv.at[1], (left, tp))
    for t in range(3):
        project(t, 1, gate)
        serve(1)
    tail.wait()
    head.wait()

    taps = taps_ref[...].astype(F32)
    step = 64
    before = rim[0, RIM - 1:RIM, :].astype(F32)

    def label(i, shift):
        return lc[WINDOW + i * step + shift:WINDOW + (i + 1) * step + shift, 0:1]

    for i in range(rows // step):
        r = slice(i * step, (i + 1) * step)
        x = value[r, :].astype(F32)
        after = (value[(i + 1) * step:(i + 1) * step + RIM, :] if (i + 1) * step < rows else rim[1, :, :])[0:1].astype(F32)
        prev = jnp.concatenate([before, x[:-1]], axis=0)
        nxt = jnp.concatenate([x[1:], after], axis=0)
        conv = (
            taps[0:1] * jnp.where(label(i, -1) == label(i, 0), prev, 0.0)
            + taps[1:2] * x
            + taps[2:3] * jnp.where(label(i, 1) == label(i, 0), nxt, 0.0)
        )
        gate[r, :] = (conv * jax.nn.sigmoid(conv) * gate[r, :].astype(F32)).astype(BF16)
        before = x[step - 1:step]
        if i % 3 == 2:
            serve(1)

    per_tp = n // ntp
    mine_rows = pl.ds(core * half, half)
    partner_rows = pl.ds((1 - core) * half, half)
    units = []
    for d in range(n):
        if d in (1, n - 1) and n > 2:
            units.append((2 * (n - 1) + 2 * (n - d), d, 0, 1))
            units.append((2 * (n - 1) + 2 * d, d, 1, 1))
        else:
            units.append((2 * (n - 1) + (2 * max(d, n - d) if d else 0), d, 0, 2))
    units.sort()

    def target(owner):
        to = owner // per_tp
        local = lax.rem(owner, per_tp)
        slot = lax.rem(tp - to + ntp, ntp) - 1
        return to, local, slot

    def lower(u):
        _, d, way, count = units[u]
        owner = place(lax.rem(pos + d, n))
        w = down[pl.ds(pl.multiple_of(owner * block + way * depth, depth), count * depth), :]

        def body(i, carry):
            r = pl.ds(pl.multiple_of(i * big, big), big)
            product = lax.dot_general(
                gate[r, :], w, (((1,), (1,)), ((), ())), preferred_element_type=F32
            ).astype(BF16)
            for j in range(count):
                pd[owner, way + j, r, :] = product[:, j * depth:(j + 1) * depth]
            return carry

        lax.fori_loop(0, 3, body, 0)
        return remote(
            pd.at[owner, pl.ds(way, count), partner_rows], box.at[owner, pl.ds(way, count)],
            down_send.at[u], down_recv.at[u], (me, partner),
        )

    def reduce(u, c):
        _, d, way, count = units[u]
        owner = place(lax.rem(pos + d, n))
        c.wait()

        def merge(i, carry):
            r = pl.ds(pl.multiple_of(i * tile, tile), tile)
            o = pl.ds(pl.multiple_of(core * half + i * tile, tile), tile)
            for j in range(way, way + count):
                pd[owner, j, o, :] = (pd[owner, j, o, :].astype(F32) + box[owner, j, r, :].astype(F32)).astype(BF16)
            return carry

        lax.fori_loop(0, half // tile, merge, 0, unroll=2)
        to, local, slot = target(owner)

        @pl.when(to != tp)
        def _():
            remote(
                pd.at[owner, pl.ds(way, count), mine_rows], inbox.at[local, slot, pl.ds(way, count)],
                out_send.at[u], out_recv.at[local, slot], (me, to),
            )

    waiting = None
    for u in range(len(units)):
        serve(units[u][0] - done[0])
        c = lower(u)
        if waiting is not None:
            reduce(*waiting)
        waiting = (u, c)
    reduce(*waiting)
    serve(len(queue))

    span = per_tp * block
    for local in range(per_tp):
        owner = tp * per_tp + local
        for slot in range(ntp - 1):
            ref = inbox.at[local, slot]
            pltpu.make_async_remote_copy(
                src_ref=ref, dst_ref=ref, send_sem=out_send.at[0], recv_sem=out_recv.at[local, slot],
                device_id=(me, partner), device_id_type=MESH,
            ).wait_recv()
        for same in range(2):
            base = (core if same else 1 - core) * half
            slots = range(1, ntp - 1, 2) if same else range(0, ntp - 1, 2)

            def finish(i, carry):
                r = pl.ds(pl.multiple_of(i * tile, tile), tile)
                o = pl.ds(pl.multiple_of(base + i * tile, tile), tile)
                kept = mixed[o, pl.ds(pl.multiple_of(tp * span, span), span)]
                for j in range(2):
                    s = sum(inbox[local, slot, j, r, :].astype(F32) for slot in slots)
                    if same:
                        s = s + pd[owner, j, o, :].astype(F32)
                    cols = slice(local * block + j * depth, local * block + (j + 1) * depth)
                    out_ref[o, cols] = (kept[:, cols].astype(F32) + s).astype(BF16)
                return carry

            lax.fori_loop(0, half // tile, finish, 0)
    for u, (_, d, way, count) in enumerate(units):
        owner = place(lax.rem(pos + d, n))
        to, local, slot = target(owner)

        @pl.when(to != tp)
        def _():
            ref = pd.at[owner, pl.ds(way, count), mine_rows]
            pltpu.make_async_remote_copy(
                src_ref=ref, dst_ref=ref, send_sem=out_send.at[u], recv_sem=out_recv.at[0, 0],
                device_id=(me, to), device_id_type=MESH,
            ).wait_send()
    for stream in range(4):
        for way in range(2):
            for s in range(n - 1):
                ring(stream, way, s, False).wait_send()


def solution(mesh):
    n, ntp = mesh.shape["sp"], mesh.shape["tp"]

    def per_device(q, k, v, sink, doc, res, wout, gain, wv, wg, taps, wd):
        rows, model = res.shape
        hidden = wv.shape[1]
        block = wv.shape[0]
        ny = ntp // 2
        labels = doc + 1
        lab_row = labels[None, :]
        vm = pl.BlockSpec(memory_space=pltpu.VMEM)
        hbm = pl.BlockSpec(memory_space=pl.ANY)
        smem = pl.BlockSpec(memory_space=pltpu.SMEM)
        dma = pltpu.SemaphoreType.DMA
        kvc = k.shape[1]
        span = model // ntp
        scratch = [
            pltpu.VMEM((2, n * block, hidden), BF16),
            pltpu.VMEM((n * block, hidden), BF16),
            pltpu.VMEM((rows + 2 * WINDOW, kvc), BF16),
            pltpu.VMEM((rows + 2 * WINDOW, kvc), BF16),
            pltpu.VMEM((1, rows + 2 * WINDOW), jnp.int32),
            pltpu.VMEM((rows + 2 * WINDOW, WINDOW), F32),
            pltpu.VMEM((rows, model), BF16),
            pltpu.VMEM((rows // 2, model), BF16),
            pltpu.VMEM((max(ny - 1, 1), rows // 2 // ny, model), BF16),
            pltpu.VMEM((rows, model), BF16),
            pltpu.VMEM((rows, model), BF16),
            pltpu.VMEM((rows, hidden), BF16),
            pltpu.VMEM((rows, hidden), BF16),
            pltpu.VMEM((2, RIM, hidden), BF16),
            pltpu.VMEM((n, 2, rows, block // 2), BF16),
            pltpu.VMEM((n, 2, rows // 2, block // 2), BF16),
            pltpu.VMEM((n // ntp, ntp - 1, 2, rows // 2, block // 2), BF16),
            pltpu.VMEM((rows // 2 // ny, model), BF16),
            dma((4,)),
            dma((4, 2, n - 1)), dma((4, 2, n - 1)),
            dma((3, 2)), dma((3, 2)),
            dma((2,)), dma((2,)),
            dma, dma,
            dma((ny,)), dma((ny,)),
            dma((ny,)), dma((ny,)),
            dma, dma,
            dma((n + 2,)), dma((n + 2,)),
            dma((n + 2,)), dma((n // ntp, ntp - 1)),
        ]
        return pl.pallas_call(
            functools.partial(kernel, n, ntp),
            out_shape=jax.ShapeDtypeStruct((rows, span), BF16),
            in_specs=[vm, vm, vm, smem, vm, hbm, vm, vm, hbm, hbm, vm, hbm],
            out_specs=vm,
            scratch_shapes=scratch,
            compiler_params=pltpu.CompilerParams(
                collective_id=0, has_side_effects=True, vmem_limit_bytes=67043328
            ),
            name="layer",
        )(q, k, v, sink, lab_row, res, wout, gain[None, :], wv, wg, taps, wd)

    placed = (
        P("sp", "tp"), P("sp", "tp"), P("sp", "tp"), P("tp"), P("sp"), P("sp", None),
        P("tp", None), P(), P("sp", "tp"), P("sp", "tp"), P(None, "tp"), P("sp", "tp"),
    )
    return jax.shard_map(
        per_device, mesh=mesh, in_specs=placed, out_specs=P("sp", "tp"), check_vma=False
    )
```

profile of v0, /device:TPU:0, one launch (start us, length us, event | category | flops | bytes accessed | tf_op | source)
XLA Modules:
  0.0 199.8 jit_solution(15652527315017378975)
XLA Ops:
  0.0 0.7 broadcast_add_fusion
  0.7 0.6 broadcast_in_dim.6.lab_row_ref
  1.3 196.4 %layer.1 = bf16[768,512]{1,0:T(8,128)(2,1)} custom-call(bf16[768,512]{1,0:T(8,128)(2,1)} %q_ref.1, bf16[768,128]{1,0:T(8,128)(2,1)} %k_ref.1, bf16[768,128]{1,0:T(8,128)(2,1)} %v_ref.1, f32[8]{0:T(128)} %sink_ref.1, s32[1,768]{1,0:T(1,128)} %broadcast_in_dim.6.lab_row_ref, bf16[768,2048]{1,0:T(8,128)(2,1)} %res_hbm.1, bf16[512,2048]{1,0:T(8,128)(2,1)} %wout_ref.1, ...), custom_call_target="tpu_custom_call" | custom-call | tf_op jit(solution)/shard_map/layer/pallas_call | solution.py:457
  197.7 2.1 %copy.14 = bf16[768,512]{1,0:T(8,128)(2,1)} copy(bf16[768,512]{1,0:T(8,128)(2,1)} %layer.1) | data formatting | bytes 1572864
where the time goes:
time: 200 us
  Pallas kernels  196 us (98%)
  local copies, waits for them, and re-layouts  2.65 us (1%)
    pallas_call x1, Pallas kernels, per_device(): pl.pallas_call(functools.partial(kernel, n, ntp), out_shape=jax.ShapeDtyp...  196 us

commit v1 on v0

--- a/solution.py
+++ b/solution.py
@@ -12,12 +12,13 @@
 EPS = 1e-06
 NEG = -1e30
 RIM = 16
+LANES = 128
 MESH = pl.DeviceIdType.MESH
 F32 = jnp.float32
 BF16 = jnp.bfloat16
 
 
-def kernel(
+def ring_kernel(
     n, ntp,
     q_ref, k_ref, v_ref, sink_ref, lab_row_ref,
     res_hbm, wout_ref, gain_ref, wv_hbm, wg_hbm, taps_ref, wd_hbm,
@@ -408,10 +409,592 @@
                 ring(stream, way, s, False).wait_send()
 
 
+def paired_kernel(
+    n, ntp,
+    q_ref, k_ref, v_ref, sink_ref, lab_row_ref,
+    res_hbm, wout_ref, gain_ref, wv_hbm, wg_hbm, taps_ref, wd_hbm,
+    out_ref,
+    w3, other, kx, vx, lx, lp, lc, same, part, first, second, mixed, normed, value, gate,
+    pd, box, yin1, zin1, zin2, yin2, res,
+    loc_sem, halo_send, halo_recv, lab_send, lab_recv, zs, zr, xs, xr,
+    core_send, core_recv, y_send, y_recv, ag_send, ag_recv, rim_send, rim_recv,
+    box_send, box_recv, yo1_send, yo1_recv, zo1_send, zo1_recv, zo2_send, zo2_recv, yo2_send, yo2_recv,
+):
+    me = lax.axis_index("sp")
+    tp = lax.axis_index("tp")
+    core = lax.rem(tp, 2)
+    y = tp // 2
+    z = me // 2
+    x = lax.rem(me, 2)
+    zh = z // 2
+    own = lax.rem(z, 2)
+    pair = 1 - own
+    zp = 2 * zh + pair
+    far_mid = 2 - zh
+    far_end = 3 - 3 * zh
+    partner = y * 2 + 1 - core
+    across = (1 - y) * 2 + core
+    beside = (zp * 2 + x, tp)
+    sibling = (z * 2 + 1 - x, tp)
+    rows, cols = q_ref.shape
+    half = rows // 2
+    piece = half // 2
+    block, hidden = wv_hbm.shape
+    wide = w3.shape[2]
+    narrow = hidden - wide
+    model = wout_ref.shape[1]
+    span = out_ref.shape[1]
+    is_mid = (z == 1) | (z == 2)
+    is_end = (z == 0) | (z == 3)
+    roles = ((is_end, narrow, wide, 0, narrow), (is_mid, wide, narrow, narrow, 0))
+
+    def copy(src, dst, send, recv, where):
+        return pltpu.make_async_remote_copy(
+            src_ref=src, dst_ref=dst, send_sem=send, recv_sem=recv, device_id=where, device_id_type=MESH
+        )
+
+    def arrive(ref, recv):
+        copy(ref, ref, core_send.at[0], recv, (me, partner)).wait_recv()
+
+    def left(ref, send):
+        copy(ref, ref, send, core_recv.at[0], (me, partner)).wait_send()
+
+    def spot(s, zo, xo, width):
+        return w3.at[s, pl.ds(pl.multiple_of((zo * 2 + xo) * block, block), block), pl.ds(0, width)]
+
+    sources = (wv_hbm, wg_hbm, wd_hbm)
+
+    def loads(s):
+        for cond, width, rest, at, rest_at in roles:
+            def pair_of():
+                a = pltpu.make_async_copy(sources[s].at[:, pl.ds(at, width)], spot(s, z, x, width), loc_sem.at[s, 0])
+                b = pltpu.make_async_copy(
+                    sources[s].at[:, pl.ds(rest_at, rest)], other.at[s, :, pl.ds(0, rest)], loc_sem.at[s, 1]
+                )
+                return a, b
+            yield cond, pair_of
+
+    for s in range(3):
+        for cond, pair_of in loads(s):
+            @pl.when(cond)
+            def _():
+                for c in pair_of():
+                    c.start()
+    my_piece = core * half + y * piece
+    res_load = pltpu.make_async_copy(res_hbm.at[pl.ds(pl.multiple_of(my_piece, piece), piece)], res, loc_sem.at[3, 0])
+    res_load.start()
+
+    barrier = pltpu.get_barrier_semaphore()
+    peers = [(lax.rem(me + j, n), tp) for j in range(1, n)] + [(me, lax.rem(tp + j, ntp)) for j in range(1, ntp)]
+    for peer in peers:
+        pl.semaphore_signal(barrier, inc=1, device_id=peer, device_id_type=MESH)
+    for s in range(3):
+        for cond, pair_of in loads(s):
+            @pl.when(cond)
+            def _():
+                for c in pair_of():
+                    c.wait()
+    res_load.wait()
+    pl.semaphore_wait(barrier, len(peers))
+
+    def begin(s):
+        @pl.when(is_end)
+        def _():
+            copy(other.at[s, :, pl.ds(0, wide)], spot(s, z, x, wide), zs.at[s, 0], zr.at[s, 0], beside).start()
+            a = spot(s, z, x, narrow)
+            copy(a, a, zs.at[s, 1], zr.at[s, 2], ((3 - z) * 2 + x, tp)).start()
+            copy(a, a, xs.at[s, 0], xr.at[s, 0], sibling).start()
+
+        @pl.when(is_mid)
+        def _():
+            a = spot(s, z, x, wide)
+            b = other.at[s, :, pl.ds(0, narrow)]
+            copy(a, a, zs.at[s, 1], zr.at[s, 1], ((3 - z) * 2 + x, tp)).start()
+            copy(b, spot(s, z, x, narrow), zs.at[s, 0], zr.at[s, 0], beside).start()
+            copy(b, spot(s, z, x, narrow), zs.at[s, 2], zr.at[s, 1], ((3 - zp) * 2 + x, tp)).start()
+            copy(a, a, xs.at[s, 0], xr.at[s, 0], sibling).start()
+
+    owners = (zp, far_mid, far_end)
+
+    def event(s, j):
+        for cond, width, _, _, _ in roles:
+            @pl.when(cond)
+            def _():
+                a = spot(s, owners[j], x, width)
+                arrive(a, zr.at[s, j])
+                copy(a, a, xs.at[s, j + 1], xr.at[s, j + 1], sibling).start()
+        if j == 0:
+            @pl.when(is_mid)
+            def _():
+                a = spot(s, zp, x, wide)
+                copy(a, a, zs.at[s, 3], zr.at[s, 2], ((3 - z) * 2 + x, tp)).start()
+
+    def xwait(s, j):
+        for cond, width, _, _, _ in roles:
+            @pl.when(cond)
+            def _():
+                arrive(spot(s, ((z,) + owners)[j], 1 - x, width), xr.at[s, j])
+
+    def finish_stream(s):
+        @pl.when(is_end)
+        def _():
+            left(spot(s, z, x, wide), zs.at[s, 0])
+            left(spot(s, z, x, narrow), zs.at[s, 1])
+            for j in range(4):
+                left(spot(s, z, x, narrow), xs.at[s, j])
+
+        @pl.when(is_mid)
+        def _():
+            left(spot(s, z, x, wide), zs.at[s, 1])
+            left(spot(s, z, x, narrow), zs.at[s, 0])
+            left(spot(s, z, x, narrow), zs.at[s, 2])
+            left(spot(s, z, x, wide), zs.at[s, 3])
+            for j in range(4):
+                left(spot(s, z, x, wide), xs.at[s, j])
+
+    right, before = lax.rem(me + 1, n), lax.rem(me + n - 1, n)
+    ends = pl.ds(rows - WINDOW, WINDOW)
+    starts = pl.ds(0, WINDOW)
+    low, high = pl.ds(0, WINDOW), pl.ds(rows + WINDOW, WINDOW)
+    halo = []
+    for i, (src, dst) in enumerate(((k_ref, kx), (v_ref, vx))):
+        halo.append(copy(src.at[ends], dst.at[low], halo_send.at[i, 0], halo_recv.at[i, 0], (right, tp)))
+        halo.append(copy(src.at[starts], dst.at[high], halo_send.at[i, 1], halo_recv.at[i, 1], (before, tp)))
+    halo.append(copy(lab_row_ref.at[:, ends], lx.at[:, low], halo_send.at[2, 0], halo_recv.at[2, 0], (right, tp)))
+    halo.append(copy(lab_row_ref.at[:, starts], lx.at[:, high], halo_send.at[2, 1], halo_recv.at[2, 1], (before, tp)))
+    for c in halo:
+        c.start()
+    begin(0)
+
+    @pl.when(is_end)
+    def _():
+        if narrow < wide:
+            w3[:, :, narrow:wide] = jnp.zeros((3, n * block, wide - narrow), BF16)
+
+    inner = pl.ds(WINDOW, rows)
+    kx[inner, :] = k_ref[...]
+    vx[inner, :] = v_ref[...]
+    lx[:, inner] = lab_row_ref[...]
+    for c in halo:
+        c.wait()
+    lx[:, low] = jnp.where(me == 0, -1, lx[:, low])
+    lx[:, high] = jnp.where(me == n - 1, -1, lx[:, high])
+    lab_copy = copy(lx, lp, lab_send, lab_recv, beside)
+    lab_copy.start()
+    chunks = rows // WINDOW
+
+    def columns(row_ref, slot):
+        for i in range(chunks + 2):
+            chunk = slice(i * WINDOW, (i + 1) * WINDOW)
+            square = jnp.broadcast_to(row_ref[0:1, chunk].astype(F32), (WINDOW, WINDOW))
+            lc[chunk, :] = jnp.transpose(square)
+        for i in range(chunks):
+            here = lc[WINDOW * (i + 1):WINDOW * (i + 2), :]
+            for side, shift in ((0, -1), (1, 1)):
+                there = lc[WINDOW * (i + 1) + shift:WINDOW * (i + 2) + shift, :]
+                same[slot, side, i * WINDOW:(i + 1) * WINDOW, :] = jnp.where(here == there, 1.0, 0.0)
+
+    columns(lx, own)
+
+    kv_local = k_ref.shape[1] // HEAD_DIM
+    per_kv = cols // k_ref.shape[1]
+    per_half = chunks // 2
+    tile = 32
+
+    def attend(i, carry):
+        own_half = i // per_half
+        j = lax.rem(i, per_half)
+        turn = (1 - y) * (per_half - 1 - j) + y * j
+        b = ((1 - own_half) * (1 - core) + own_half * core) * per_half + turn
+        here = pl.ds(pl.multiple_of(b * WINDOW, WINDOW), WINDOW)
+        wide_keys = pl.ds(pl.multiple_of(b * WINDOW, WINDOW), 3 * WINDOW)
+        q = q_ref[here, :]
+        kw = kx[wide_keys, :]
+        vw = vx[wide_keys, :]
+        lab_k = lx[0:1, wide_keys].astype(F32)
+        lab_q = lc[pl.ds(pl.multiple_of(b * WINDOW + WINDOW, WINDOW), WINDOW), 0:1]
+        key = lax.broadcasted_iota(jnp.int32, (WINDOW, 3 * WINDOW), 1) - WINDOW
+        query = lax.broadcasted_iota(jnp.int32, (WINDOW, 3 * WINDOW), 0)
+        allowed = (jnp.abs(key - query) <= WINDOW) & (lab_q == lab_k)
+        results = []
+        for g in range(kv_local):
+            k = kw[:, g * HEAD_DIM:(g + 1) * HEAD_DIM]
+            v = vw[:, g * HEAD_DIM:(g + 1) * HEAD_DIM]
+            for u in range(per_kv):
+                h = g * per_kv + u
+                qh = q[:, h * HEAD_DIM:(h + 1) * HEAD_DIM]
+                score = lax.dot_general(
+                    qh, k, (((1,), (1,)), ((), ())), preferred_element_type=F32
+                ) * HEAD_DIM ** (-0.5)
+                score = jnp.where(allowed, score, NEG)
+                sink = sink_ref[h]
+                highest = jnp.maximum(jnp.max(score, axis=1, keepdims=True), sink)
+                raw = jnp.where(allowed, jnp.exp(score - highest), 0.0)
+                total = jnp.sum(raw, axis=1, keepdims=True) + jnp.exp(sink - highest)
+                probs = (raw / total).astype(BF16)
+                results.append(jnp.dot(probs, v, preferred_element_type=F32).astype(BF16))
+        attended = jnp.concatenate(results, axis=1)
+        part[here, :] = jnp.dot(attended, wout_ref[...], preferred_element_type=F32).astype(BF16)
+        mine = first.at[pl.ds(pl.multiple_of(turn * WINDOW, WINDOW), WINDOW)]
+
+        @pl.when(own_half == 0)
+        def _():
+            copy(part.at[here], mine, core_send.at[j], core_recv.at[j], (me, partner)).start()
+
+        @pl.when(own_half == 1)
+        def _():
+            arrive(mine, core_recv.at[j])
+
+            def add(t, carry):
+                r = pl.ds(pl.multiple_of(turn * WINDOW + t * tile, tile), tile)
+                o = pl.ds(pl.multiple_of(b * WINDOW + t * tile, tile), tile)
+                first[r, :] = (part[o, :].astype(F32) + first[r, :].astype(F32)).astype(BF16)
+                return carry
+
+            lax.fori_loop(0, WINDOW // tile, add, 0)
+
+        @pl.when(i == per_half)
+        def _():
+            y_copy(0, y).start()
+
+        @pl.when(i == per_half + 1)
+        def _():
+            y_copy(1, y).start()
+
+        @pl.when(i == 1)
+        def _():
+            event(0, 0)
+            begin(1)
+
+        @pl.when(i == 3)
+        def _():
+            event(0, 1)
+
+        return carry
+
+    def y_copy(k, yy):
+        if k == 0:
+            count, src, dst = 2 * piece // 3, (1 - yy) * (half - 2 * piece // 3), (1 - yy) * (piece // 3)
+        else:
+            count, src, dst = piece // 3, 2 * piece // 3 + (1 - yy) * (piece // 3), yy * (2 * piece // 3)
+        return copy(
+            first.at[pl.ds(pl.multiple_of(src, 64), count)], second.at[pl.ds(pl.multiple_of(dst, 64), count)],
+            y_send.at[k], y_recv.at[k], (me, across),
+        )
+
+    lax.fori_loop(0, 2 * per_half, attend, 0)
+    event(1, 0)
+    event(0, 2)
+    lab_copy.wait()
+    columns(lp, pair)
+    for k in range(2):
+        y_copy(k, 1 - y).wait_recv()
+
+    def norm(slot, start, count):
+        def body(i, carry):
+            r = pl.ds(pl.multiple_of(start + i * tile, tile), tile)
+            m = mixed[r, :].astype(F32)
+            mean_sq = jnp.mean(m * m, axis=1, keepdims=True)
+            normed[slot, r, :] = (m * lax.rsqrt(mean_sq + EPS) * gain_ref[...]).astype(BF16)
+            return carry
+
+        lax.fori_loop(0, count // tile, body, 0)
+
+    def add_second(i, carry):
+        r = pl.ds(pl.multiple_of(i * tile, tile), tile)
+        f = pl.ds(pl.multiple_of(y * piece + i * tile, tile), tile)
+        o = pl.ds(pl.multiple_of(my_piece + i * tile, tile), tile)
+        s = first[f, :].astype(F32) + second[r, :].astype(F32)
+        mixed[o, :] = (res[r, :].astype(F32) + s).astype(BF16)
+        return carry
+
+    lax.fori_loop(0, piece // tile, add_second, 0)
+
+    def part_of(c, yy):
+        return c * half + yy * piece
+
+    def mixed_at(c, yy):
+        return mixed.at[pl.ds(pl.multiple_of(part_of(c, yy), piece), piece)]
+
+    def normed_at(slot, c, yy):
+        return normed.at[slot, pl.ds(pl.multiple_of(part_of(c, yy), piece), piece)]
+
+    def share(k, ref, where):
+        copy(ref, ref, ag_send.at[k], ag_recv.at[k], where).start()
+
+    share(0, mixed_at(core, y), (me, across))
+    share(1, mixed_at(core, y), (me, partner))
+    norm(own, my_piece, piece)
+    share(2, normed_at(own, core, y), beside)
+    begin(2)
+    event(1, 1)
+    arrive(mixed_at(1 - core, y), ag_recv.at[1])
+    norm(own, part_of(1 - core, y), piece)
+    arrive(mixed_at(core, 1 - y), ag_recv.at[0])
+    share(3, mixed_at(core, 1 - y), (me, partner))
+    norm(own, part_of(core, 1 - y), piece)
+    arrive(normed_at(pair, core, y), ag_recv.at[2])
+    share(4, normed_at(pair, core, y), (me, across))
+    share(5, normed_at(pair, core, y), (me, partner))
+    arrive(mixed_at(1 - core, 1 - y), ag_recv.at[3])
+    norm(own, part_of(1 - core, 1 - y), piece)
+
+    big = rows // 3
+
+    def project(which, slot):
+        def body(t, carry):
+            r = pl.ds(pl.multiple_of(t * big, big), big)
+            product = jnp.dot(normed[slot, r, :], w3[which], preferred_element_type=F32).astype(BF16)
+            if which == 0:
+                value[slot, pl.ds(pl.multiple_of(RIM + t * big, RIM), big), :] = product
+            else:
+                gate[slot, r, :] = product
+            return carry
+
+        lax.fori_loop(0, 3, body, 0)
+
+    for j in range(4):
+        xwait(0, j)
+    project(0, own)
+    event(1, 2)
+    event(2, 0)
+    arrive(normed_at(pair, core, 1 - y), ag_recv.at[4])
+    share(6, normed_at(pair, core, 1 - y), (me, partner))
+    for j in range(4):
+        xwait(1, j)
+    project(1, own)
+    arrive(normed_at(pair, 1 - core, y), ag_recv.at[5])
+    arrive(normed_at(pair, 1 - core, 1 - y), ag_recv.at[6])
+    project(0, pair)
+
+    inside = pl.ds(RIM, RIM)
+    last = pl.ds(rows, RIM)
+    fronts, backs = pl.ds(0, RIM), pl.ds(RIM + rows, RIM)
+    facing = ((3 - z) * 2 + 1 - x, tp)
+    rims = (
+        (x == 0, ((0, last, 0, fronts, sibling), (1, inside, 0, backs, sibling),
+                  (1, last, 1, fronts, sibling), (0, inside, 1, backs, facing))),
+        (x == 1, ((0, inside, 0, backs, sibling), (0, last, 1, fronts, sibling),
+                  (1, inside, 1, backs, sibling), (1, last, 0, fronts, facing))),
+    )
+    for cond, sends in rims:
+        @pl.when(cond)
+        def _():
+            for frm, rs, to, rd, where in sends:
+                pad = 2 * to + (0 if rd is fronts else 1)
+                copy(value.at[frm, rs], value.at[to, rd], rim_send.at[pad], rim_recv.at[pad], where).start()
+
+    project(1, pair)
+    event(2, 1)
+    for slot in range(2):
+        for side, rd in enumerate((fronts, backs)):
+            arrive(value.at[slot, rd], rim_recv.at[2 * slot + side])
+
+    taps_all = taps_ref[...].astype(F32)
+    taps = jnp.where(is_mid, taps_all[:, narrow:], taps_all[:, :wide])
+    step = 64
+    lanes = wide // WINDOW
+
+    for slot in range(2):
+        def gated(i, carry):
+            base = i * step
+            r = pl.ds(pl.multiple_of(base, step), step)
+            x_rows = value[slot, pl.ds(pl.multiple_of(RIM + base, RIM), step), :].astype(F32)
+            above = value[slot, pl.ds(pl.multiple_of(base, RIM), RIM), :].astype(F32)[RIM - 1:RIM]
+            below = value[slot, pl.ds(pl.multiple_of(RIM + base + step, RIM), RIM), :].astype(F32)[0:1]
+            prev = jnp.concatenate([above, x_rows[:-1]], axis=0)
+            nxt = jnp.concatenate([x_rows[1:], below], axis=0)
+            with_prev = jnp.concatenate([same[slot, 0, r, :]] * lanes, axis=1) > 0.5
+            with_next = jnp.concatenate([same[slot, 1, r, :]] * lanes, axis=1) > 0.5
+            conv = (
+                taps[0:1] * jnp.where(with_prev, prev, 0.0)
+                + taps[1:2] * x_rows
+                + taps[2:3] * jnp.where(with_next, nxt, 0.0)
+            )
+            gate[slot, r, :] = (conv * jax.nn.sigmoid(conv) * gate[slot, r, :].astype(F32)).astype(BF16)
+            return carry
+
+        lax.fori_loop(0, rows // step, gated, 0)
+
+    order = (1 + zh, 3 * zh, far_mid, far_end)
+    quarter = rows // 2
+
+    def lower(u):
+        t = order[u]
+        w = w3[2, pl.ds(pl.multiple_of(t * span, span), span), :]
+        for slot in range(2):
+            def body(i, carry):
+                r = pl.ds(pl.multiple_of(i * big, big), big)
+                pd[u, slot, r, :] = lax.dot_general(
+                    gate[slot, r, :], w, (((1,), (1,)), ((), ())), preferred_element_type=F32
+                ).astype(BF16)
+                return carry
+
+            lax.fori_loop(0, 3, body, 0)
+
+        @pl.when(core != lax.rem(t, 2))
+        def _():
+            copy(pd.at[u], box.at[u // 2], box_send.at[u], box_recv.at[u // 2], (me, partner)).start()
+
+    def rows_of(ref, at):
+        return ref.at[pl.ds(at, quarter)]
+
+    def merge(count, body):
+        def step_rows(i, carry):
+            body(pl.ds(pl.multiple_of(i * tile, tile), tile), pl.ds(pl.multiple_of(quarter + i * tile, tile), tile))
+            return carry
+
+        lax.fori_loop(0, count // tile, step_rows, 0)
+
+    upper, under = pl.ds(0, quarter), pl.ds(quarter, quarter)
+
+    def stage_one(u):
+        t = order[u]
+        target_y = t // 2
+
+        @pl.when(core == lax.rem(t, 2))
+        def _():
+            arrive(box.at[u // 2], box_recv.at[u // 2])
+
+            def add(slot, lo):
+                def body(i, carry):
+                    r = pl.ds(pl.multiple_of(lo + i * tile, tile), tile)
+                    pd[u, slot, r, :] = (
+                        pd[u, slot, r, :].astype(F32) + box[u // 2, slot, r, :].astype(F32)
+                    ).astype(BF16)
+                    return carry
+
+                lax.fori_loop(0, quarter // tile, body, 0)
+
+            add(pair, quarter)
+            copy(pd.at[u, pair, under], zin1.at[u // 2], zo1_send.at[u // 2], zo1_recv.at[u // 2], beside).start()
+            add(0, 0)
+            add(1, 0)
+
+            @pl.when(y != target_y)
+            def _():
+                copy(pd.at[u, :, upper], yin1, yo1_send, yo1_recv, (me, across)).start()
+
+            add(own, quarter)
+
+    def stage_two(u):
+        t = order[u]
+        target_y = t // 2
+
+        @pl.when(core == lax.rem(t, 2))
+        def _():
+            @pl.when(y == target_y)
+            def _():
+                arrive(yin1, yo1_recv)
+
+                def body(slot):
+                    def inner_body(i, carry):
+                        r = pl.ds(pl.multiple_of(i * tile, tile), tile)
+                        pd[u, slot, r, :] = (
+                            pd[u, slot, r, :].astype(F32) + yin1[slot, r, :].astype(F32)
+                        ).astype(BF16)
+                        return carry
+
+                    lax.fori_loop(0, quarter // tile, inner_body, 0)
+
+                body(pair)
+                copy(pd.at[u, pair, upper], zin2, zo2_send, zo2_recv, beside).start()
+                body(own)
+
+            arrive(zin1.at[u // 2], zo1_recv.at[u // 2])
+
+            def add(i, carry):
+                r = pl.ds(pl.multiple_of(i * tile, tile), tile)
+                o = pl.ds(pl.multiple_of(quarter + i * tile, tile), tile)
+                pd[u, own, o, :] = (
+                    pd[u, own, o, :].astype(F32) + zin1[u // 2, r, :].astype(F32)
+                ).astype(BF16)
+                return carry
+
+            lax.fori_loop(0, quarter // tile, add, 0)
+
+            @pl.when(y != target_y)
+            def _():
+                copy(pd.at[u, own, under], yin2, yo2_send, yo2_recv, (me, across)).start()
+
+    def stage_three(u):
+        t = order[u]
+
+        @pl.when(tp == t)
+        def _():
+            arrive(zin2, zo2_recv)
+            arrive(yin2, yo2_recv)
+            for at, extra in ((0, zin2), (quarter, yin2)):
+                def body(i, carry):
+                    r = pl.ds(pl.multiple_of(i * tile, tile), tile)
+                    o = pl.ds(pl.multiple_of(at + i * tile, tile), tile)
+                    kept = mixed[o, pl.ds(pl.multiple_of(t * span, span), span)].astype(F32)
+                    s = pd[u, own, o, :].astype(F32) + extra[r, :].astype(F32)
+                    out_ref[o, :] = (kept + s).astype(BF16)
+                    return carry
+
+                lax.fori_loop(0, quarter // tile, body, 0)
+
+    def drain(u):
+        t = order[u]
+
+        @pl.when(core != lax.rem(t, 2))
+        def _():
+            left(pd.at[u], box_send.at[u])
+
+        @pl.when(core == lax.rem(t, 2))
+        def _():
+            left(pd.at[u, pair, under], zo1_send.at[u // 2])
+
+            @pl.when(y != t // 2)
+            def _():
+                left(pd.at[u, :, upper], yo1_send)
+                left(pd.at[u, own, under], yo2_send)
+
+            @pl.when(y == t // 2)
+            def _():
+                left(pd.at[u, pair, upper], zo2_send)
+
+    xwait(2, 0)
+    xwait(2, 1)
+    lower(0)
+    lower(1)
+    stage_one(0)
+    stage_one(1)
+    event(2, 2)
+    xwait(2, 2)
+    lower(2)
+    stage_two(0)
+    stage_two(1)
+    stage_one(2)
+    xwait(2, 3)
+    lower(3)
+    stage_one(3)
+    stage_three(0)
+    stage_three(1)
+    stage_two(2)
+    stage_two(3)
+    stage_three(2)
+    stage_three(3)
+
+    for s in range(3):
+        finish_stream(s)
+    for j in range(per_half):
+        left(first.at[pl.ds(0, WINDOW)], core_send.at[j])
+    for k in range(2):
+        y_copy(k, y).wait_send()
+    for k in range(7):
+        left(mixed_at(core, y), ag_send.at[k])
+    for pad in range(4):
+        left(value.at[0, fronts], rim_send.at[pad])
+    for u in range(4):
+        drain(u)
+
+
 def solution(mesh):
     n, ntp = mesh.shape["sp"], mesh.shape["tp"]
 
-    def per_device(q, k, v, sink, doc, res, wout, gain, wv, wg, taps, wd):
+    def by_ring(q, k, v, sink, doc, res, wout, gain, wv, wg, taps, wd):
         rows, model = res.shape
         hidden = wv.shape[1]
         block = wv.shape[0]
@@ -455,7 +1038,7 @@
             dma((n + 2,)), dma((n // ntp, ntp - 1)),
         ]
         return pl.pallas_call(
-            functools.partial(kernel, n, ntp),
+            functools.partial(ring_kernel, n, ntp),
             out_shape=jax.ShapeDtypeStruct((rows, span), BF16),
             in_specs=[vm, vm, vm, smem, vm, hbm, vm, vm, hbm, hbm, vm, hbm],
             out_specs=vm,
@@ -466,10 +1049,74 @@
             name="layer",
         )(q, k, v, sink, lab_row, res, wout, gain[None, :], wv, wg, taps, wd)
 
+
+    def by_pairs(q, k, v, sink, doc, res, wout, gain, wv, wg, taps, wd):
+        rows, model = res.shape
+        block, hidden = wv.shape
+        half = rows // 2
+        piece = half // 2
+        span = model // ntp
+        kvc = k.shape[1]
+        wide = (hidden // LANES + 1) // 2 * LANES
+        lab_row = (doc + 1)[None, :]
+        vm = pl.BlockSpec(memory_space=pltpu.VMEM)
+        hbm = pl.BlockSpec(memory_space=pl.ANY)
+        smem = pl.BlockSpec(memory_space=pltpu.SMEM)
+        dma = pltpu.SemaphoreType.DMA
+        scratch = [
+            pltpu.VMEM((3, n * block, wide), BF16),
+            pltpu.VMEM((3, block, wide), BF16),
+            pltpu.VMEM((rows + 2 * WINDOW, kvc), BF16),
+            pltpu.VMEM((rows + 2 * WINDOW, kvc), BF16),
+            pltpu.VMEM((1, rows + 2 * WINDOW), jnp.int32),
+            pltpu.VMEM((1, rows + 2 * WINDOW), jnp.int32),
+            pltpu.VMEM((rows + 2 * WINDOW, WINDOW), F32),
+            pltpu.VMEM((2, 2, rows, WINDOW), F32),
+            pltpu.VMEM((rows, model), BF16),
+            pltpu.VMEM((half, model), BF16),
+            pltpu.VMEM((piece, model), BF16),
+            pltpu.VMEM((rows, model), BF16),
+            pltpu.VMEM((2, rows, model), BF16),
+            pltpu.VMEM((2, rows + 2 * RIM, wide), BF16),
+            pltpu.VMEM((2, rows, wide), BF16),
+            pltpu.VMEM((4, 2, rows, span), BF16),
+            pltpu.VMEM((2, 2, rows, span), BF16),
+            pltpu.VMEM((2, half, span), BF16),
+            pltpu.VMEM((2, half, span), BF16),
+            pltpu.VMEM((half, span), BF16),
+            pltpu.VMEM((half, span), BF16),
+            pltpu.VMEM((piece, model), BF16),
+            dma((4, 2)),
+            dma((3, 2)), dma((3, 2)),
+            dma, dma,
+            dma((3, 4)), dma((3, 3)),
+            dma((3, 4)), dma((3, 4)),
+            dma((rows // WINDOW // 2,)), dma((rows // WINDOW // 2,)),
+            dma((2,)), dma((2,)),
+            dma((7,)), dma((7,)),
+            dma((4,)), dma((4,)),
+            dma((4,)), dma((2,)),
+            dma, dma,
+            dma((2,)), dma((2,)),
+            dma, dma,
+            dma, dma,
+        ]
+        return pl.pallas_call(
+            functools.partial(paired_kernel, n, ntp),
+            out_shape=jax.ShapeDtypeStruct((rows, span), BF16),
+            in_specs=[vm, vm, vm, smem, vm, hbm, vm, vm, hbm, hbm, vm, hbm],
+            out_specs=vm,
+            scratch_shapes=scratch,
+            compiler_params=pltpu.CompilerParams(
+                collective_id=0, has_side_effects=True, vmem_limit_bytes=67043328
+            ),
+            name="layer",
+        )(q, k, v, sink, lab_row, res, wout, gain[None, :], wv, wg, taps, wd)
+
     placed = (
         P("sp", "tp"), P("sp", "tp"), P("sp", "tp"), P("tp"), P("sp"), P("sp", None),
         P("tp", None), P(), P("sp", "tp"), P("sp", "tp"), P(None, "tp"), P("sp", "tp"),
     )
     return jax.shard_map(
-        per_device, mesh=mesh, in_specs=placed, out_specs=P("sp", "tp"), check_vma=False
+        by_pairs if (n, ntp) == (8, 4) else by_ring, mesh=mesh, in_specs=placed, out_specs=P("sp", "tp"), check_vma=False
     )

time: 200 us -> 171 us (0.85)
  the two profiles are of different devices: /device:TPU:0 before, /device:TPU:16 now
where the time goes in v1:
time: 171 us
  Pallas kernels  168 us (98%)
  local copies, waits for them, and re-layouts  2.65 us (2%)
    pallas_call x1, Pallas kernels, by_pairs(): pl.pallas_call(functools.partial(paired_kernel, n, ntp), out_shape=jax.Sh...  168 us

profile of v1, /device:TPU:16, one launch (start us, length us, event | category | flops | bytes accessed | tf_op | source)
XLA Modules:
  0.0 171.2 jit_solution(14647728190482201720)
XLA Ops:
  0.0 0.7 broadcast_add_fusion
  0.7 0.6 broadcast_in_dim.6.lab_row_ref
  1.3 167.8 %layer.1 = bf16[768,512]{1,0:T(8,128)(2,1)} custom-call(bf16[768,512]{1,0:T(8,128)(2,1)} %q_ref.1, bf16[768,128]{1,0:T(8,128)(2,1)} %k_ref.1, bf16[768,128]{1,0:T(8,128)(2,1)} %v_ref.1, f32[8]{0:T(128)} %sink_ref.1, s32[1,768]{1,0:T(1,128)} %broadcast_in_dim.6.lab_row_ref, bf16[768,2048]{1,0:T(8,128)(2,1)} %res_hbm.1, bf16[512,2048]{1,0:T(8,128)(2,1)} %wout_ref.1, ...), custom_call_target="tpu_custom_call" | custom-call | tf_op jit(solution)/shard_map/layer/pallas_call | solution.py:1104
  169.1 2.1 %copy.14 = bf16[768,512]{1,0:T(8,128)(2,1)} copy(bf16[768,512]{1,0:T(8,128)(2,1)} %layer.1) | data formatting | bytes 1572864

commit v2 on v1

--- a/solution.py
+++ b/solution.py
@@ -411,11 +411,11 @@
 
 def paired_kernel(
     n, ntp,
-    q_ref, k_ref, v_ref, sink_ref, lab_row_ref,
-    res_hbm, wout_ref, gain_ref, wv_hbm, wg_hbm, taps_ref, wd_hbm,
+    q_hbm, k_ref, v_ref, sink_ref, lab_row_ref,
+    res_hbm, wout_hbm, gain_ref, wv_hbm, wg_hbm, taps_ref, wd_hbm,
     out_ref,
     w3, other, kx, vx, lx, lp, lc, same, part, first, second, mixed, normed, value, gate,
-    pd, box, yin1, zin1, zin2, yin2, res,
+    pd, box, yin1, zin1, zin2, yin2, res, q_ref, wout_ref,
     loc_sem, halo_send, halo_recv, lab_send, lab_recv, zs, zr, xs, xr,
     core_send, core_recv, y_send, y_recv, ag_send, ag_recv, rim_send, rim_recv,
     box_send, box_recv, yo1_send, yo1_recv, zo1_send, zo1_recv, zo2_send, zo2_recv, yo2_send, yo2_recv,
@@ -436,17 +436,20 @@
     across = (1 - y) * 2 + core
     beside = (zp * 2 + x, tp)
     sibling = (z * 2 + 1 - x, tp)
-    rows, cols = q_ref.shape
+    rows, cols = q_hbm.shape
     half = rows // 2
     piece = half // 2
     block, hidden = wv_hbm.shape
     wide = w3.shape[2]
     narrow = hidden - wide
-    model = wout_ref.shape[1]
+    model = wout_hbm.shape[1]
     span = out_ref.shape[1]
     is_mid = (z == 1) | (z == 2)
     is_end = (z == 0) | (z == 3)
-    roles = ((is_end, narrow, wide, 0, narrow), (is_mid, wide, narrow, narrow, 0))
+    is_wide = is_mid
+    is_narrow = is_end
+    roles = ((is_narrow, narrow, wide, 0, narrow), (is_wide, wide, narrow, narrow, 0))
+    sides = (is_end, is_mid)
 
     def copy(src, dst, send, recv, where):
         return pltpu.make_async_remote_copy(
@@ -483,51 +486,80 @@
     my_piece = core * half + y * piece
     res_load = pltpu.make_async_copy(res_hbm.at[pl.ds(pl.multiple_of(my_piece, piece), piece)], res, loc_sem.at[3, 0])
     res_load.start()
+    late_loads = (
+        pltpu.make_async_copy(q_hbm, q_ref, loc_sem.at[4, 0]),
+        pltpu.make_async_copy(wout_hbm, wout_ref, loc_sem.at[4, 1]),
+    )
+    for c in late_loads:
+        c.start()
 
     barrier = pltpu.get_barrier_semaphore()
     peers = [(lax.rem(me + j, n), tp) for j in range(1, n)] + [(me, lax.rem(tp + j, ntp)) for j in range(1, ntp)]
     for peer in peers:
         pl.semaphore_signal(barrier, inc=1, device_id=peer, device_id_type=MESH)
-    for s in range(3):
+
+    def loaded(s):
         for cond, pair_of in loads(s):
             @pl.when(cond)
             def _():
                 for c in pair_of():
                     c.wait()
-    res_load.wait()
+
+    loaded(0)
     pl.semaphore_wait(barrier, len(peers))
 
-    def begin(s):
-        @pl.when(is_end)
-        def _():
-            copy(other.at[s, :, pl.ds(0, wide)], spot(s, z, x, wide), zs.at[s, 0], zr.at[s, 0], beside).start()
-            a = spot(s, z, x, narrow)
-            copy(a, a, zs.at[s, 1], zr.at[s, 2], ((3 - z) * 2 + x, tp)).start()
-            copy(a, a, xs.at[s, 0], xr.at[s, 0], sibling).start()
-
-        @pl.when(is_mid)
-        def _():
-            a = spot(s, z, x, wide)
-            b = other.at[s, :, pl.ds(0, narrow)]
-            copy(a, a, zs.at[s, 1], zr.at[s, 1], ((3 - z) * 2 + x, tp)).start()
-            copy(b, spot(s, z, x, narrow), zs.at[s, 0], zr.at[s, 0], beside).start()
-            copy(b, spot(s, z, x, narrow), zs.at[s, 2], zr.at[s, 1], ((3 - zp) * 2 + x, tp)).start()
-            copy(a, a, xs.at[s, 0], xr.at[s, 0], sibling).start()
+    def begin_end(s):
+        for cond, width, rest, _, _ in roles:
+            @pl.when(is_end & cond)
+            def _():
+                b = other.at[s, :, pl.ds(0, rest)]
+                copy(b, spot(s, z, x, rest), zs.at[s, 0], zr.at[s, 0], beside).start()
+
+    def begin_far(s):
+        for cond, width, rest, _, _ in roles:
+            @pl.when(is_end & cond)
+            def _():
+                a = spot(s, z, x, width)
+                copy(a, a, zs.at[s, 1], zr.at[s, 2], ((3 - z) * 2 + x, tp)).start()
+
+            @pl.when(is_mid & cond)
+            def _():
+                b = other.at[s, :, pl.ds(0, rest)]
+                copy(b, spot(s, z, x, rest), zs.at[s, 2], zr.at[s, 1], ((3 - zp) * 2 + x, tp)).start()
+
+    def begin_mid(s):
+        for cond, width, rest, _, _ in roles:
+            @pl.when(is_mid & cond)
+            def _():
+                a = spot(s, z, x, width)
+                copy(a, a, zs.at[s, 1], zr.at[s, 1], ((3 - z) * 2 + x, tp)).start()
+
+    def begin_out(s):
+        for cond, width, rest, _, _ in roles:
+            @pl.when(is_mid & cond)
+            def _():
+                b = other.at[s, :, pl.ds(0, rest)]
+                copy(b, spot(s, z, x, rest), zs.at[s, 0], zr.at[s, 0], beside).start()
+
+    def begin_x(s, who=(0, 1)):
+        for (cond, width, _, _, _), side in ((r, sides[w]) for r in roles for w in who):
+            @pl.when(cond & side)
+            def _():
+                a = spot(s, z, x, width)
+                copy(a, a, xs.at[s, 0], xr.at[s, 0], sibling).start()
 
     owners = (zp, far_mid, far_end)
 
-    def event(s, j):
-        for cond, width, _, _, _ in roles:
-            @pl.when(cond)
-            def _():
-                a = spot(s, owners[j], x, width)
-                arrive(a, zr.at[s, j])
-                copy(a, a, xs.at[s, j + 1], xr.at[s, j + 1], sibling).start()
-        if j == 0:
-            @pl.when(is_mid)
-            def _():
-                a = spot(s, zp, x, wide)
-                copy(a, a, zs.at[s, 3], zr.at[s, 2], ((3 - z) * 2 + x, tp)).start()
+    def event(s, j, who=(0, 1)):
+        for side in who:
+            for cond, width, _, _, _ in roles:
+                @pl.when(sides[side] & cond)
+                def _():
+                    a = spot(s, owners[j], x, width)
+                    arrive(a, zr.at[s, j])
+                    if side == 1 and j == 0:
+                        copy(a, a, zs.at[s, 3], zr.at[s, 2], ((3 - z) * 2 + x, tp)).start()
+                    copy(a, a, xs.at[s, j + 1], xr.at[s, j + 1], sibling).start()
 
     def xwait(s, j):
         for cond, width, _, _, _ in roles:
@@ -536,21 +568,18 @@
                 arrive(spot(s, ((z,) + owners)[j], 1 - x, width), xr.at[s, j])
 
     def finish_stream(s):
-        @pl.when(is_end)
-        def _():
-            left(spot(s, z, x, wide), zs.at[s, 0])
-            left(spot(s, z, x, narrow), zs.at[s, 1])
-            for j in range(4):
-                left(spot(s, z, x, narrow), xs.at[s, j])
-
-        @pl.when(is_mid)
-        def _():
-            left(spot(s, z, x, wide), zs.at[s, 1])
-            left(spot(s, z, x, narrow), zs.at[s, 0])
-            left(spot(s, z, x, narrow), zs.at[s, 2])
-            left(spot(s, z, x, wide), zs.at[s, 3])
-            for j in range(4):
-                left(spot(s, z, x, wide), xs.at[s, j])
+        for cond, width, rest, _, _ in roles:
+            @pl.when(cond)
+            def _():
+                left(spot(s, z, x, rest), zs.at[s, 0])
+                left(spot(s, z, x, width), zs.at[s, 1])
+                for j in range(4):
+                    left(spot(s, z, x, width), xs.at[s, j])
+
+            @pl.when(is_mid & cond)
+            def _():
+                left(spot(s, z, x, rest), zs.at[s, 2])
+                left(spot(s, z, x, width), zs.at[s, 3])
 
     right, before = lax.rem(me + 1, n), lax.rem(me + n - 1, n)
     ends = pl.ds(rows - WINDOW, WINDOW)
@@ -564,9 +593,18 @@
     halo.append(copy(lab_row_ref.at[:, starts], lx.at[:, high], halo_send.at[2, 1], halo_recv.at[2, 1], (before, tp)))
     for c in halo:
         c.start()
-    begin(0)
-
-    @pl.when(is_end)
+    begin_end(0)
+    begin_mid(0)
+    begin_out(0)
+    begin_far(0)
+    begin_x(0)
+    loaded(1)
+    begin_end(1)
+    begin_x(1)
+    loaded(2)
+    begin_x(2, (0,))
+
+    @pl.when(is_narrow)
     def _():
         if narrow < wide:
             w3[:, :, narrow:wide] = jnp.zeros((3, n * block, wide - narrow), BF16)
@@ -575,26 +613,32 @@
     kx[inner, :] = k_ref[...]
     vx[inner, :] = v_ref[...]
     lx[:, inner] = lab_row_ref[...]
-    for c in halo:
-        c.wait()
-    lx[:, low] = jnp.where(me == 0, -1, lx[:, low])
-    lx[:, high] = jnp.where(me == n - 1, -1, lx[:, high])
     lab_copy = copy(lx, lp, lab_send, lab_recv, beside)
-    lab_copy.start()
     chunks = rows // WINDOW
 
-    def columns(row_ref, slot):
-        for i in range(chunks + 2):
+    def columns(row_ref, which):
+        for i in which:
             chunk = slice(i * WINDOW, (i + 1) * WINDOW)
             square = jnp.broadcast_to(row_ref[0:1, chunk].astype(F32), (WINDOW, WINDOW))
             lc[chunk, :] = jnp.transpose(square)
+
+    def neighbours(slot):
         for i in range(chunks):
             here = lc[WINDOW * (i + 1):WINDOW * (i + 2), :]
             for side, shift in ((0, -1), (1, 1)):
                 there = lc[WINDOW * (i + 1) + shift:WINDOW * (i + 2) + shift, :]
                 same[slot, side, i * WINDOW:(i + 1) * WINDOW, :] = jnp.where(here == there, 1.0, 0.0)
 
-    columns(lx, own)
+    columns(lx, range(1, chunks + 1))
+
+    def edges():
+        for c in halo:
+            c.wait()
+        lx[:, low] = jnp.where(me == 0, -1, lx[:, low])
+        lx[:, high] = jnp.where(me == n - 1, -1, lx[:, high])
+        lab_copy.start()
+        columns(lx, (0, chunks + 1))
+        neighbours(own)
 
     kv_local = k_ref.shape[1] // HEAD_DIM
     per_kv = cols // k_ref.shape[1]
@@ -604,11 +648,12 @@
     def attend(i, carry):
         own_half = i // per_half
         j = lax.rem(i, per_half)
-        turn = (1 - y) * (per_half - 1 - j) + y * j
+        flip = (1 - own_half) * core + own_half * (1 - y)
+        turn = flip * (per_half - 1 - j) + (1 - flip) * j
         b = ((1 - own_half) * (1 - core) + own_half * core) * per_half + turn
         here = pl.ds(pl.multiple_of(b * WINDOW, WINDOW), WINDOW)
         wide_keys = pl.ds(pl.multiple_of(b * WINDOW, WINDOW), 3 * WINDOW)
-        q = q_ref[here, :]
+        q = q_ref[here, :] * jnp.asarray(HEAD_DIM ** (-0.5), BF16)
         kw = kx[wide_keys, :]
         vw = vx[wide_keys, :]
         lab_k = lx[0:1, wide_keys].astype(F32)
@@ -620,30 +665,31 @@
         for g in range(kv_local):
             k = kw[:, g * HEAD_DIM:(g + 1) * HEAD_DIM]
             v = vw[:, g * HEAD_DIM:(g + 1) * HEAD_DIM]
-            for u in range(per_kv):
-                h = g * per_kv + u
-                qh = q[:, h * HEAD_DIM:(h + 1) * HEAD_DIM]
-                score = lax.dot_general(
-                    qh, k, (((1,), (1,)), ((), ())), preferred_element_type=F32
-                ) * HEAD_DIM ** (-0.5)
-                score = jnp.where(allowed, score, NEG)
+            heads = range(g * per_kv, (g + 1) * per_kv)
+            stacked = jnp.concatenate([q[:, h * HEAD_DIM:(h + 1) * HEAD_DIM] for h in heads], axis=0)
+            scores = lax.dot_general(stacked, k, (((1,), (1,)), ((), ())), preferred_element_type=F32)
+            raws, scales = [], []
+            for u, h in enumerate(heads):
+                score = jnp.where(allowed, scores[u * WINDOW:(u + 1) * WINDOW], NEG)
                 sink = sink_ref[h]
                 highest = jnp.maximum(jnp.max(score, axis=1, keepdims=True), sink)
-                raw = jnp.where(allowed, jnp.exp(score - highest), 0.0)
-                total = jnp.sum(raw, axis=1, keepdims=True) + jnp.exp(sink - highest)
-                probs = (raw / total).astype(BF16)
-                results.append(jnp.dot(probs, v, preferred_element_type=F32).astype(BF16))
+                raw = jnp.exp(score - highest)
+                scales.append(1.0 / (jnp.sum(raw, axis=1, keepdims=True) + jnp.exp(sink - highest)))
+                raws.append(raw.astype(BF16))
+            summed = jnp.dot(jnp.concatenate(raws, axis=0), v, preferred_element_type=F32)
+            for u in range(per_kv):
+                results.append((summed[u * WINDOW:(u + 1) * WINDOW] * scales[u]).astype(BF16))
         attended = jnp.concatenate(results, axis=1)
         part[here, :] = jnp.dot(attended, wout_ref[...], preferred_element_type=F32).astype(BF16)
         mine = first.at[pl.ds(pl.multiple_of(turn * WINDOW, WINDOW), WINDOW)]
 
         @pl.when(own_half == 0)
         def _():
-            copy(part.at[here], mine, core_send.at[j], core_recv.at[j], (me, partner)).start()
+            copy(part.at[here], mine, core_send.at[turn], core_recv.at[turn], (me, partner)).start()
 
         @pl.when(own_half == 1)
         def _():
-            arrive(mine, core_recv.at[j])
+            arrive(mine, core_recv.at[turn])
 
             def add(t, carry):
                 r = pl.ds(pl.multiple_of(turn * WINDOW + t * tile, tile), tile)
@@ -663,12 +709,17 @@
 
         @pl.when(i == 1)
         def _():
-            event(0, 0)
-            begin(1)
+            edges()
 
         @pl.when(i == 3)
         def _():
-            event(0, 1)
+            event(0, 0, (1,))
+            begin_mid(1)
+            begin_out(1)
+
+        @pl.when(i == 4)
+        def _():
+            event(0, 1, (1,))
 
         return carry
 
@@ -682,11 +733,10 @@
             y_send.at[k], y_recv.at[k], (me, across),
         )
 
+    res_load.wait()
+    for c in late_loads:
+        c.wait()
     lax.fori_loop(0, 2 * per_half, attend, 0)
-    event(1, 0)
-    event(0, 2)
-    lab_copy.wait()
-    columns(lp, pair)
     for k in range(2):
         y_copy(k, 1 - y).wait_recv()
 
@@ -716,8 +766,10 @@
     def mixed_at(c, yy):
         return mixed.at[pl.ds(pl.multiple_of(part_of(c, yy), piece), piece)]
 
-    def normed_at(slot, c, yy):
-        return normed.at[slot, pl.ds(pl.multiple_of(part_of(c, yy), piece), piece)]
+    bit = piece // 2
+
+    def normed_at(slot, c, yy, b):
+        return normed.at[slot, pl.ds(pl.multiple_of(part_of(c, yy) + b * bit, bit), bit)]
 
     def share(k, ref, where):
         copy(ref, ref, ag_send.at[k], ag_recv.at[k], where).start()
@@ -725,18 +777,31 @@
     share(0, mixed_at(core, y), (me, across))
     share(1, mixed_at(core, y), (me, partner))
     norm(own, my_piece, piece)
-    share(2, normed_at(own, core, y), beside)
-    begin(2)
-    event(1, 1)
+    for b in range(2):
+        share(4 + b, normed_at(own, core, y, b), beside)
+    event(0, 0, (0,))
+    event(1, 0, (1,))
+    event(0, 1, (0,))
     arrive(mixed_at(1 - core, y), ag_recv.at[1])
     norm(own, part_of(1 - core, y), piece)
+    event(0, 2, (1,))
     arrive(mixed_at(core, 1 - y), ag_recv.at[0])
-    share(3, mixed_at(core, 1 - y), (me, partner))
+    share(2, mixed_at(core, 1 - y), (me, partner))
     norm(own, part_of(core, 1 - y), piece)
-    arrive(normed_at(pair, core, y), ag_recv.at[2])
-    share(4, normed_at(pair, core, y), (me, across))
-    share(5, normed_at(pair, core, y), (me, partner))
-    arrive(mixed_at(1 - core, 1 - y), ag_recv.at[3])
+    event(0, 2, (0,))
+    begin_far(1)
+
+    def serve_spread(b):
+        arrive(normed_at(pair, core, y, b), ag_recv.at[4 + b])
+        share(6 + b, normed_at(pair, core, y, b), (me, across))
+        share(8 + b, normed_at(pair, core, y, b), (me, partner))
+
+    serve_spread(0)
+    serve_spread(1)
+    event(1, 1, (1,))
+    event(1, 0, (0,))
+    begin_end(2)
+    arrive(mixed_at(1 - core, 1 - y), ag_recv.at[2])
     norm(own, part_of(1 - core, 1 - y), piece)
 
     big = rows // 3
@@ -753,45 +818,89 @@
 
         lax.fori_loop(0, 3, body, 0)
 
-    for j in range(4):
-        xwait(0, j)
-    project(0, own)
-    event(1, 2)
-    event(2, 0)
-    arrive(normed_at(pair, core, 1 - y), ag_recv.at[4])
-    share(6, normed_at(pair, core, 1 - y), (me, partner))
-    for j in range(4):
-        xwait(1, j)
-    project(1, own)
-    arrive(normed_at(pair, 1 - core, y), ag_recv.at[5])
-    arrive(normed_at(pair, 1 - core, 1 - y), ag_recv.at[6])
-    project(0, pair)
-
     inside = pl.ds(RIM, RIM)
     last = pl.ds(rows, RIM)
     fronts, backs = pl.ds(0, RIM), pl.ds(RIM + rows, RIM)
     facing = ((3 - z) * 2 + 1 - x, tp)
-    rims = (
-        (x == 0, ((0, last, 0, fronts, sibling), (1, inside, 0, backs, sibling),
-                  (1, last, 1, fronts, sibling), (0, inside, 1, backs, facing))),
-        (x == 1, ((0, inside, 0, backs, sibling), (0, last, 1, fronts, sibling),
-                  (1, inside, 1, backs, sibling), (1, last, 0, fronts, facing))),
+    near_rims = (
+        (x == 0, ((0, last, 0, 0), (1, inside, 0, 1), (1, last, 1, 0))),
+        (x == 1, ((0, inside, 0, 1), (0, last, 1, 0), (1, inside, 1, 1))),
     )
-    for cond, sends in rims:
+    far_rims = (((x == 0) & (zh == 1), (0, inside, 1, 1)), ((x == 1) & (zh == 0), (1, last, 0, 0)))
+
+    def rim_copy(frm, source, to, side, where):
+        target = value.at[to, (fronts, backs)[side]]
+        pad = 2 * to + side
+        copy(value.at[frm, source], target, rim_send.at[pad], rim_recv.at[pad], where).start()
+
+    def send_far_rims(side):
+        for cond, spec in far_rims:
+            @pl.when(cond & side)
+            def _():
+                rim_copy(*spec, facing)
+
+    def serve_x(s):
+        for j in range(4):
+            xwait(s, j)
+
+    serve_x(0)
+    project(0, own)
+    send_far_rims(is_mid)
+    begin_mid(2)
+    event(1, 1, (0,))
+    event(1, 2)
+
+    def serve_diagonal(b):
+        arrive(normed_at(pair, core, 1 - y, b), ag_recv.at[6 + b])
+        share(10 + b, normed_at(pair, core, 1 - y, b), (me, partner))
+
+    def serve_rest(b):
+        arrive(normed_at(pair, 1 - core, y, b), ag_recv.at[8 + b])
+        arrive(normed_at(pair, 1 - core, 1 - y, b), ag_recv.at[10 + b])
+
+    serve_diagonal(0)
+    serve_diagonal(1)
+    serve_rest(0)
+    serve_rest(1)
+    project(0, pair)
+
+    send_far_rims(is_end)
+    for cond, specs in near_rims:
         @pl.when(cond)
         def _():
-            for frm, rs, to, rd, where in sends:
-                pad = 2 * to + (0 if rd is fronts else 1)
-                copy(value.at[frm, rs], value.at[to, rd], rim_send.at[pad], rim_recv.at[pad], where).start()
-
+            for spec in specs:
+                rim_copy(*spec, sibling)
+
+    begin_out(2)
+    begin_far(2)
+    begin_x(2, (1,))
+    event(2, 0, (1,))
+    serve_x(1)
+    project(1, own)
     project(1, pair)
-    event(2, 1)
-    for slot in range(2):
+    event(2, 0, (0,))
+    lab_copy.wait()
+    columns(lp, range(chunks + 2))
+    neighbours(pair)
+
+    def serve_rims(slot):
         for side, rd in enumerate((fronts, backs)):
-            arrive(value.at[slot, rd], rim_recv.at[2 * slot + side])
+            if slot == side:
+                @pl.when((x != side) | (zh != side))
+                def _():
+                    arrive(value.at[slot, rd], rim_recv.at[2 * slot + side])
+
+                @pl.when((x == side) & (zh == side))
+                def _():
+                    value[slot, rd, :] = jnp.zeros((RIM, wide), BF16)
+            else:
+                arrive(value.at[slot, rd], rim_recv.at[2 * slot + side])
+
+    serve_rims(0)
+    serve_rims(1)
 
     taps_all = taps_ref[...].astype(F32)
-    taps = jnp.where(is_mid, taps_all[:, narrow:], taps_all[:, :wide])
+    taps = jnp.where(is_wide, taps_all[:, narrow:], taps_all[:, :wide])
     step = 64
     lanes = wide // WINDOW
 
@@ -816,7 +925,7 @@
 
         lax.fori_loop(0, rows // step, gated, 0)
 
-    order = (1 + zh, 3 * zh, far_mid, far_end)
+    order = (z, zp, far_mid, far_end)
     quarter = rows // 2
 
     def lower(u):
@@ -824,107 +933,123 @@
         w = w3[2, pl.ds(pl.multiple_of(t * span, span), span), :]
         for slot in range(2):
             def body(i, carry):
-                r = pl.ds(pl.multiple_of(i * big, big), big)
+                r = pl.ds(pl.multiple_of(i * quarter, quarter), quarter)
                 pd[u, slot, r, :] = lax.dot_general(
                     gate[slot, r, :], w, (((1,), (1,)), ((), ())), preferred_element_type=F32
                 ).astype(BF16)
                 return carry
 
-            lax.fori_loop(0, 3, body, 0)
+            lax.fori_loop(0, 2, body, 0)
 
         @pl.when(core != lax.rem(t, 2))
         def _():
             copy(pd.at[u], box.at[u // 2], box_send.at[u], box_recv.at[u // 2], (me, partner)).start()
 
-    def rows_of(ref, at):
-        return ref.at[pl.ds(at, quarter)]
-
-    def merge(count, body):
-        def step_rows(i, carry):
-            body(pl.ds(pl.multiple_of(i * tile, tile), tile), pl.ds(pl.multiple_of(quarter + i * tile, tile), tile))
+    cuts = (quarter, quarter, rows // 6, rows // 6)
+
+    def segment(u, g):
+        count = (rows - cuts[u]) // 2
+        return cuts[u] + g * count, count
+
+    def accumulate(ref, slot, at, count, other_ref, base):
+        def body(i, carry):
+            r = pl.ds(pl.multiple_of(at + i * tile, tile), tile)
+            o = pl.ds(pl.multiple_of(base + i * tile, tile), tile)
+            ref[slot, r, :] = (ref[slot, r, :].astype(F32) + other_ref[o, :].astype(F32)).astype(BF16)
             return carry
 
-        lax.fori_loop(0, count // tile, step_rows, 0)
-
-    upper, under = pl.ds(0, quarter), pl.ds(quarter, quarter)
+        lax.fori_loop(0, count // tile, body, 0)
+
+    def z_first(u, g):
+        at, count = segment(u, g)
+        return copy(
+            pd.at[u, pair, pl.ds(at, count)], zin1.at[u // 2, g, pl.ds(0, count)],
+            zo1_send.at[u // 2, g], zo1_recv.at[u // 2, g], beside,
+        )
+
+    def then_y(u, g):
+        at, count = segment(u, g)
+        return copy(
+            pd.at[u, own, pl.ds(at, count)], yin2.at[g, pl.ds(0, count)], yo2_send.at[g], yo2_recv.at[g], (me, across)
+        )
+
+    def y_first(u, slot, k):
+        top = pl.ds(0, cuts[u])
+        return copy(pd.at[u, slot, top], yin1.at[slot, top], yo1_send.at[k], yo1_recv.at[k], (me, across))
+
+    def then_z(u):
+        top = pl.ds(0, cuts[u])
+        return copy(pd.at[u, pair, top], zin2.at[top], zo2_send, zo2_recv, beside)
 
     def stage_one(u):
         t = order[u]
-        target_y = t // 2
 
         @pl.when(core == lax.rem(t, 2))
         def _():
             arrive(box.at[u // 2], box_recv.at[u // 2])
 
-            def add(slot, lo):
-                def body(i, carry):
-                    r = pl.ds(pl.multiple_of(lo + i * tile, tile), tile)
-                    pd[u, slot, r, :] = (
-                        pd[u, slot, r, :].astype(F32) + box[u // 2, slot, r, :].astype(F32)
-                    ).astype(BF16)
-                    return carry
-
-                lax.fori_loop(0, quarter // tile, body, 0)
-
-            add(pair, quarter)
-            copy(pd.at[u, pair, under], zin1.at[u // 2], zo1_send.at[u // 2], zo1_recv.at[u // 2], beside).start()
-            add(0, 0)
-            add(1, 0)
-
-            @pl.when(y != target_y)
-            def _():
-                copy(pd.at[u, :, upper], yin1, yo1_send, yo1_recv, (me, across)).start()
-
-            add(own, quarter)
-
-    def stage_two(u):
+            def add(slot, at, count):
+                accumulate(pd.at[u], slot, at, count, box.at[u // 2, slot], at)
+
+            def tops():
+                add(pair, 0, cuts[u])
+
+                @pl.when(y != t // 2)
+                def _():
+                    y_first(u, pair, 0).start()
+
+                add(own, 0, cuts[u])
+
+                @pl.when(y != t // 2)
+                def _():
+                    y_first(u, own, 1).start()
+
+            def rest():
+                for g in range(2):
+                    add(pair, *segment(u, g))
+                    z_first(u, g).start()
+
+            if u < 2:
+                tops()
+                rest()
+            else:
+                rest()
+                tops()
+            for g in range(2):
+                add(own, *segment(u, g))
+
+    def stage_y(u):
         t = order[u]
-        target_y = t // 2
+
+        @pl.when(tp == t)
+        def _():
+            top = pl.ds(0, cuts[u])
+            arrive(yin1.at[pair, top], yo1_recv.at[0])
+            accumulate(pd.at[u], pair, 0, cuts[u], yin1.at[pair], 0)
+            then_z(u).start()
+            arrive(yin1.at[own, top], yo1_recv.at[1])
+            accumulate(pd.at[u], own, 0, cuts[u], yin1.at[own], 0)
+
+    def stage_z(u):
+        t = order[u]
 
         @pl.when(core == lax.rem(t, 2))
         def _():
-            @pl.when(y == target_y)
-            def _():
-                arrive(yin1, yo1_recv)
-
-                def body(slot):
-                    def inner_body(i, carry):
-                        r = pl.ds(pl.multiple_of(i * tile, tile), tile)
-                        pd[u, slot, r, :] = (
-                            pd[u, slot, r, :].astype(F32) + yin1[slot, r, :].astype(F32)
-                        ).astype(BF16)
-                        return carry
-
-                    lax.fori_loop(0, quarter // tile, inner_body, 0)
-
-                body(pair)
-                copy(pd.at[u, pair, upper], zin2, zo2_send, zo2_recv, beside).start()
-                body(own)
-
-            arrive(zin1.at[u // 2], zo1_recv.at[u // 2])
-
-            def add(i, carry):
-                r = pl.ds(pl.multiple_of(i * tile, tile), tile)
-                o = pl.ds(pl.multiple_of(quarter + i * tile, tile), tile)
-                pd[u, own, o, :] = (
-                    pd[u, own, o, :].astype(F32) + zin1[u // 2, r, :].astype(F32)
-                ).astype(BF16)
-                return carry
-
-            lax.fori_loop(0, quarter // tile, add, 0)
-
-            @pl.when(y != target_y)
-            def _():
-                copy(pd.at[u, own, under], yin2, yo2_send, yo2_recv, (me, across)).start()
+            for g in range(2):
+                at, count = segment(u, g)
+                arrive(zin1.at[u // 2, g, pl.ds(0, count)], zo1_recv.at[u // 2, g])
+                accumulate(pd.at[u], own, at, count, zin1.at[u // 2, g], 0)
+
+                @pl.when(y != t // 2)
+                def _():
+                    then_y(u, g).start()
 
     def stage_three(u):
         t = order[u]
 
         @pl.when(tp == t)
         def _():
-            arrive(zin2, zo2_recv)
-            arrive(yin2, yo2_recv)
-            for at, extra in ((0, zin2), (quarter, yin2)):
+            def close(at, count, extra):
                 def body(i, carry):
                     r = pl.ds(pl.multiple_of(i * tile, tile), tile)
                     o = pl.ds(pl.multiple_of(at + i * tile, tile), tile)
@@ -933,7 +1058,14 @@
                     out_ref[o, :] = (kept + s).astype(BF16)
                     return carry
 
-                lax.fori_loop(0, quarter // tile, body, 0)
+                lax.fori_loop(0, count // tile, body, 0)
+
+            arrive(zin2.at[pl.ds(0, cuts[u])], zo2_recv)
+            close(0, cuts[u], zin2)
+            for g in range(2):
+                at, count = segment(u, g)
+                arrive(yin2.at[g, pl.ds(0, count)], yo2_recv.at[g])
+                close(at, count, yin2.at[g])
 
     def drain(u):
         t = order[u]
@@ -944,36 +1076,44 @@
 
         @pl.when(core == lax.rem(t, 2))
         def _():
-            left(pd.at[u, pair, under], zo1_send.at[u // 2])
+            for g in range(2):
+                z_first(u, g).wait_send()
 
             @pl.when(y != t // 2)
             def _():
-                left(pd.at[u, :, upper], yo1_send)
-                left(pd.at[u, own, under], yo2_send)
+                for k, slot in enumerate((pair, own)):
+                    y_first(u, slot, k).wait_send()
+                for g in range(2):
+                    then_y(u, g).wait_send()
 
             @pl.when(y == t // 2)
             def _():
-                left(pd.at[u, pair, upper], zo2_send)
+                then_z(u).wait_send()
 
     xwait(2, 0)
+    lower(0)
+    event(2, 1)
     xwait(2, 1)
-    lower(0)
     lower(1)
     stage_one(0)
     stage_one(1)
     event(2, 2)
     xwait(2, 2)
     lower(2)
-    stage_two(0)
-    stage_two(1)
     stage_one(2)
     xwait(2, 3)
     lower(3)
     stage_one(3)
+    stage_z(0)
+    stage_z(1)
+    stage_y(0)
+    stage_y(1)
+    stage_z(2)
+    stage_z(3)
+    stage_y(2)
+    stage_y(3)
     stage_three(0)
     stage_three(1)
-    stage_two(2)
-    stage_two(3)
     stage_three(2)
     stage_three(3)
 
@@ -983,10 +1123,16 @@
         left(first.at[pl.ds(0, WINDOW)], core_send.at[j])
     for k in range(2):
         y_copy(k, y).wait_send()
-    for k in range(7):
+    for k in range(3):
         left(mixed_at(core, y), ag_send.at[k])
+    for k in range(4, 12):
+        left(normed_at(own, core, y, 0), ag_send.at[k])
     for pad in range(4):
-        left(value.at[0, fronts], rim_send.at[pad])
+        sends = (x == pad // 3) | (zh == pad // 3) if pad in (0, 3) else x >= 0
+
+        @pl.when(sends)
+        def _():
+            left(value.at[0, fronts], rim_send.at[pad])
     for u in range(4):
         drain(u)
 
@@ -1057,8 +1203,9 @@
         piece = half // 2
         span = model // ntp
         kvc = k.shape[1]
+        third = rows // 12 * 5
         wide = (hidden // LANES + 1) // 2 * LANES
-        lab_row = (doc + 1)[None, :]
+        lab_row = doc[None, :]
         vm = pl.BlockSpec(memory_space=pltpu.VMEM)
         hbm = pl.BlockSpec(memory_space=pl.ANY)
         smem = pl.BlockSpec(memory_space=pltpu.SMEM)
@@ -1082,29 +1229,31 @@
             pltpu.VMEM((4, 2, rows, span), BF16),
             pltpu.VMEM((2, 2, rows, span), BF16),
             pltpu.VMEM((2, half, span), BF16),
-            pltpu.VMEM((2, half, span), BF16),
+            pltpu.VMEM((2, 2, third, span), BF16),
             pltpu.VMEM((half, span), BF16),
-            pltpu.VMEM((half, span), BF16),
+            pltpu.VMEM((2, third, span), BF16),
             pltpu.VMEM((piece, model), BF16),
-            dma((4, 2)),
+            pltpu.VMEM(q.shape, BF16),
+            pltpu.VMEM(wout.shape, BF16),
+            dma((5, 2)),
             dma((3, 2)), dma((3, 2)),
             dma, dma,
             dma((3, 4)), dma((3, 3)),
             dma((3, 4)), dma((3, 4)),
             dma((rows // WINDOW // 2,)), dma((rows // WINDOW // 2,)),
             dma((2,)), dma((2,)),
-            dma((7,)), dma((7,)),
+            dma((12,)), dma((12,)),
             dma((4,)), dma((4,)),
             dma((4,)), dma((2,)),
+            dma((2,)), dma((2,)),
+            dma((2, 2)), dma((2, 2)),
             dma, dma,
             dma((2,)), dma((2,)),
-            dma, dma,
-            dma, dma,
         ]
         return pl.pallas_call(
             functools.partial(paired_kernel, n, ntp),
             out_shape=jax.ShapeDtypeStruct((rows, span), BF16),
-            in_specs=[vm, vm, vm, smem, vm, hbm, vm, vm, hbm, hbm, vm, hbm],
+            in_specs=[hbm, vm, vm, smem, vm, hbm, hbm, vm, hbm, hbm, vm, hbm],
             out_specs=vm,
             scratch_shapes=scratch,
             compiler_params=pltpu.CompilerParams(

time: 171 us -> 149 us (0.87)
  Pallas kernels: 168 us -> 145 us
    pallas_call x1, Pallas kernels: 168 us -> 145 us  [by_pairs(): pl.pallas_call(functools.partial(paired_kernel, n, ntp), out_shape=jax.Sh...]
where the time goes in v2:
time: 149 us
  Pallas kernels  145 us (97%)
  local copies, waits for them, and re-layouts  3.33 us (2%)
    pallas_call x1, Pallas kernels, by_pairs(): pl.pallas_call(functools.partial(paired_kernel, n, ntp), out_shape=jax.Sh...  145 us

profile of v2, /device:TPU:16, one launch (start us, length us, event | category | flops | bytes accessed | tf_op | source)
XLA Modules:
  0.0 148.6 jit_solution(5522105857007485495)
XLA Ops:
  0.0 1.3 broadcast_in_dim.6.lab_row_ref
  1.3 145.2 %layer.1 = bf16[768,512]{1,0:T(8,128)(2,1)} custom-call(bf16[768,512]{1,0:T(8,128)(2,1)} %q_hbm.1, bf16[768,128]{1,0:T(8,128)(2,1)} %k_ref.1, bf16[768,128]{1,0:T(8,128)(2,1)} %v_ref.1, f32[8]{0:T(128)} %sink_ref.1, s32[1,768]{1,0:T(1,128)} %broadcast_in_dim.6.lab_row_ref, bf16[768,2048]{1,0:T(8,128)(2,1)} %res_hbm.1, bf16[512,2048]{1,0:T(8,128)(2,1)} %wout_hbm.1, ...), custom_call_target="tpu_custom_call" | custom-call | tf_op jit(solution)/shard_map/layer/pallas_call | solution.py:1253
  146.5 2.1 %copy.14 = bf16[768,512]{1,0:T(8,128)(2,1)} copy(bf16[768,512]{1,0:T(8,128)(2,1)} %layer.1) | data formatting | bytes 1572864

commit v3 on v2

--- a/solution.py
+++ b/solution.py
@@ -413,12 +413,12 @@
     n, ntp,
     q_hbm, k_ref, v_ref, sink_ref, lab_row_ref,
     res_hbm, wout_hbm, gain_ref, wv_hbm, wg_hbm, taps_ref, wd_hbm,
-    out_ref,
+    out_hbm,
     w3, other, kx, vx, lx, lp, lc, same, part, first, second, mixed, normed, value, gate,
-    pd, box, yin1, zin1, zin2, yin2, res, q_ref, wout_ref,
+    pd, box, yin1, zin1, zin2, yin2, res, q_ref, wout_ref, kept, result,
     loc_sem, halo_send, halo_recv, lab_send, lab_recv, zs, zr, xs, xr,
     core_send, core_recv, y_send, y_recv, ag_send, ag_recv, rim_send, rim_recv,
-    box_send, box_recv, yo1_send, yo1_recv, zo1_send, zo1_recv, zo2_send, zo2_recv, yo2_send, yo2_recv,
+    box_send, box_recv, yo1_send, yo1_recv, zo1_send, zo1_recv, zo2_send, zo2_recv, yo2_send, yo2_recv, out_sem,
 ):
     me = lax.axis_index("sp")
     tp = lax.axis_index("tp")
@@ -443,7 +443,7 @@
     wide = w3.shape[2]
     narrow = hidden - wide
     model = wout_hbm.shape[1]
-    span = out_ref.shape[1]
+    span = out_hbm.shape[1]
     is_mid = (z == 1) | (z == 2)
     is_end = (z == 0) | (z == 3)
     is_wide = is_mid
@@ -515,13 +515,15 @@
                 b = other.at[s, :, pl.ds(0, rest)]
                 copy(b, spot(s, z, x, rest), zs.at[s, 0], zr.at[s, 0], beside).start()
 
-    def begin_far(s):
+    def far_end_sends(s):
         for cond, width, rest, _, _ in roles:
             @pl.when(is_end & cond)
             def _():
                 a = spot(s, z, x, width)
                 copy(a, a, zs.at[s, 1], zr.at[s, 2], ((3 - z) * 2 + x, tp)).start()
 
+    def far_mid_sends(s):
+        for cond, width, rest, _, _ in roles:
             @pl.when(is_mid & cond)
             def _():
                 b = other.at[s, :, pl.ds(0, rest)]
@@ -596,7 +598,8 @@
     begin_end(0)
     begin_mid(0)
     begin_out(0)
-    begin_far(0)
+    far_end_sends(0)
+    far_mid_sends(0)
     begin_x(0)
     loaded(1)
     begin_end(1)
@@ -716,6 +719,7 @@
             event(0, 0, (1,))
             begin_mid(1)
             begin_out(1)
+            far_mid_sends(1)
 
         @pl.when(i == 4)
         def _():
@@ -789,17 +793,18 @@
     share(2, mixed_at(core, 1 - y), (me, partner))
     norm(own, part_of(core, 1 - y), piece)
     event(0, 2, (0,))
-    begin_far(1)
 
     def serve_spread(b):
         arrive(normed_at(pair, core, y, b), ag_recv.at[4 + b])
         share(6 + b, normed_at(pair, core, y, b), (me, across))
         share(8 + b, normed_at(pair, core, y, b), (me, partner))
 
+    event(1, 0, (0,))
+    far_end_sends(1)
+    event(1, 1, (0,))
     serve_spread(0)
     serve_spread(1)
     event(1, 1, (1,))
-    event(1, 0, (0,))
     begin_end(2)
     arrive(mixed_at(1 - core, 1 - y), ag_recv.at[2])
     norm(own, part_of(1 - core, 1 - y), piece)
@@ -839,6 +844,10 @@
             def _():
                 rim_copy(*spec, facing)
 
+    mine = mixed.at[:, pl.ds(pl.multiple_of(tp * span, span), span)]
+    kept_copy = pltpu.make_async_copy(mine, kept, loc_sem.at[3, 1])
+    kept_copy.start()
+
     def serve_x(s):
         for j in range(4):
             xwait(s, j)
@@ -847,7 +856,8 @@
     project(0, own)
     send_far_rims(is_mid)
     begin_mid(2)
-    event(1, 1, (0,))
+    begin_out(2)
+    far_mid_sends(2)
     event(1, 2)
 
     def serve_diagonal(b):
@@ -871,14 +881,14 @@
             for spec in specs:
                 rim_copy(*spec, sibling)
 
-    begin_out(2)
-    begin_far(2)
+    far_end_sends(2)
     begin_x(2, (1,))
-    event(2, 0, (1,))
+    event(2, 0, (0,))
     serve_x(1)
     project(1, own)
+    event(2, 0, (1,))
     project(1, pair)
-    event(2, 0, (0,))
+    event(2, 1, (1,))
     lab_copy.wait()
     columns(lp, range(chunks + 2))
     neighbours(pair)
@@ -928,10 +938,14 @@
     order = (z, zp, far_mid, far_end)
     quarter = rows // 2
 
+    def boxed(u, k):
+        slot = (pair, own)[k]
+        return copy(pd.at[u, slot], box.at[u // 2, slot], box_send.at[u, k], box_recv.at[u // 2, k], (me, partner))
+
     def lower(u):
         t = order[u]
         w = w3[2, pl.ds(pl.multiple_of(t * span, span), span), :]
-        for slot in range(2):
+        for k, slot in enumerate((pair, own)):
             def body(i, carry):
                 r = pl.ds(pl.multiple_of(i * quarter, quarter), quarter)
                 pd[u, slot, r, :] = lax.dot_general(
@@ -941,24 +955,26 @@
 
             lax.fori_loop(0, 2, body, 0)
 
-        @pl.when(core != lax.rem(t, 2))
-        def _():
-            copy(pd.at[u], box.at[u // 2], box_send.at[u], box_recv.at[u // 2], (me, partner)).start()
-
-    cuts = (quarter, quarter, rows // 6, rows // 6)
+            @pl.when(core != lax.rem(t, 2))
+            def _():
+                boxed(u, k).start()
+
+    cuts = (rows // 6 * 3, rows // 6 * 3, rows // 6 * 3, rows // 6 * 2)
 
     def segment(u, g):
         count = (rows - cuts[u]) // 2
         return cuts[u] + g * count, count
 
+    slab = rows // 12
+
     def accumulate(ref, slot, at, count, other_ref, base):
         def body(i, carry):
-            r = pl.ds(pl.multiple_of(at + i * tile, tile), tile)
-            o = pl.ds(pl.multiple_of(base + i * tile, tile), tile)
+            r = pl.ds(pl.multiple_of(at + i * slab, slab), slab)
+            o = pl.ds(pl.multiple_of(base + i * slab, slab), slab)
             ref[slot, r, :] = (ref[slot, r, :].astype(F32) + other_ref[o, :].astype(F32)).astype(BF16)
             return carry
 
-        lax.fori_loop(0, count // tile, body, 0)
+        lax.fori_loop(0, count // slab, body, 0)
 
     def z_first(u, g):
         at, count = segment(u, g)
@@ -986,35 +1002,35 @@
 
         @pl.when(core == lax.rem(t, 2))
         def _():
-            arrive(box.at[u // 2], box_recv.at[u // 2])
 
             def add(slot, at, count):
                 accumulate(pd.at[u], slot, at, count, box.at[u // 2, slot], at)
 
-            def tops():
+            arrive(box.at[u // 2, pair], box_recv.at[u // 2, 0])
+            if u < 3:
                 add(pair, 0, cuts[u])
 
                 @pl.when(y != t // 2)
                 def _():
                     y_first(u, pair, 0).start()
 
-                add(own, 0, cuts[u])
+            for g in range(2):
+                add(pair, *segment(u, g))
+                z_first(u, g).start()
+            if u == 3:
+                add(pair, 0, cuts[u])
 
                 @pl.when(y != t // 2)
                 def _():
-                    y_first(u, own, 1).start()
-
-            def rest():
-                for g in range(2):
-                    add(pair, *segment(u, g))
-                    z_first(u, g).start()
-
-            if u < 2:
-                tops()
-                rest()
-            else:
-                rest()
-                tops()
+                    y_first(u, pair, 0).start()
+
+            arrive(box.at[u // 2, own], box_recv.at[u // 2, 1])
+            add(own, 0, cuts[u])
+
+            @pl.when(y != t // 2)
+            def _():
+                y_first(u, own, 1).start()
+
             for g in range(2):
                 add(own, *segment(u, g))
 
@@ -1044,35 +1060,43 @@
                 def _():
                     then_y(u, g).start()
 
+    def put(at, count, k):
+        r = pl.ds(at, count)
+        return pltpu.make_async_copy(result.at[r], out_hbm.at[r], out_sem.at[k])
+
     def stage_three(u):
         t = order[u]
 
         @pl.when(tp == t)
         def _():
-            def close(at, count, extra):
+            def close(at, count, extra, k):
                 def body(i, carry):
-                    r = pl.ds(pl.multiple_of(i * tile, tile), tile)
-                    o = pl.ds(pl.multiple_of(at + i * tile, tile), tile)
-                    kept = mixed[o, pl.ds(pl.multiple_of(t * span, span), span)].astype(F32)
+                    r = pl.ds(pl.multiple_of(i * slab, slab), slab)
+                    o = pl.ds(pl.multiple_of(at + i * slab, slab), slab)
                     s = pd[u, own, o, :].astype(F32) + extra[r, :].astype(F32)
-                    out_ref[o, :] = (kept + s).astype(BF16)
+                    result[o, :] = (kept[o, :].astype(F32) + s).astype(BF16)
                     return carry
 
-                lax.fori_loop(0, count // tile, body, 0)
+                lax.fori_loop(0, count // slab, body, 0)
+                put(at, count, k).start()
 
             arrive(zin2.at[pl.ds(0, cuts[u])], zo2_recv)
-            close(0, cuts[u], zin2)
+            close(0, cuts[u], zin2, 0)
             for g in range(2):
                 at, count = segment(u, g)
                 arrive(yin2.at[g, pl.ds(0, count)], yo2_recv.at[g])
-                close(at, count, yin2.at[g])
+                close(at, count, yin2.at[g], 1 + g)
+            put(0, cuts[u], 0).wait()
+            for g in range(2):
+                put(*segment(u, g), 1 + g).wait()
 
     def drain(u):
         t = order[u]
 
         @pl.when(core != lax.rem(t, 2))
         def _():
-            left(pd.at[u], box_send.at[u])
+            for k in range(2):
+                boxed(u, k).wait_send()
 
         @pl.when(core == lax.rem(t, 2))
         def _():
@@ -1092,10 +1116,10 @@
 
     xwait(2, 0)
     lower(0)
-    event(2, 1)
+    event(2, 1, (0,))
+    stage_one(0)
     xwait(2, 1)
     lower(1)
-    stage_one(0)
     stage_one(1)
     event(2, 2)
     xwait(2, 2)
@@ -1112,6 +1136,7 @@
     stage_z(3)
     stage_y(2)
     stage_y(3)
+    kept_copy.wait()
     stage_three(0)
     stage_three(1)
     stage_three(2)
@@ -1235,6 +1260,8 @@
             pltpu.VMEM((piece, model), BF16),
             pltpu.VMEM(q.shape, BF16),
             pltpu.VMEM(wout.shape, BF16),
+            pltpu.VMEM((rows, span), BF16),
+            pltpu.VMEM((rows, span), BF16),
             dma((5, 2)),
             dma((3, 2)), dma((3, 2)),
             dma, dma,
@@ -1244,17 +1271,18 @@
             dma((2,)), dma((2,)),
             dma((12,)), dma((12,)),
             dma((4,)), dma((4,)),
-            dma((4,)), dma((2,)),
+            dma((4, 2)), dma((2, 2)),
             dma((2,)), dma((2,)),
             dma((2, 2)), dma((2, 2)),
             dma, dma,
             dma((2,)), dma((2,)),
+            dma((3,)),
         ]
         return pl.pallas_call(
             functools.partial(paired_kernel, n, ntp),
             out_shape=jax.ShapeDtypeStruct((rows, span), BF16),
             in_specs=[hbm, vm, vm, smem, vm, hbm, hbm, vm, hbm, hbm, vm, hbm],
-            out_specs=vm,
+            out_specs=hbm,
             scratch_shapes=scratch,
             compiler_params=pltpu.CompilerParams(
                 collective_id=0, has_side_effects=True, vmem_limit_bytes=67043328

time: 149 us -> 141 us (0.946)
  Pallas kernels: 145 us -> 137 us
    pallas_call x1, Pallas kernels: 145 us -> 137 us  [by_pairs(): pl.pallas_call(functools.partial(paired_kernel, n, ntp), out_shape=jax.Sh...]
where the time goes in v3:
time: 141 us; the launch traced here: 140 us
  Pallas kernels  137 us (97%)
  local copies, waits for them, and re-layouts  3.33 us (2%)
    pallas_call x1, Pallas kernels, by_pairs(): pl.pallas_call(functools.partial(paired_kernel, n, ntp), out_shape=jax.Sh...  137 us

profile of v3, /device:TPU:16, one launch (start us, length us, event | category | flops | bytes accessed | tf_op | source)
XLA Modules:
  0.0 140.2 jit_solution(4750041114243296241)
XLA Ops:
  0.0 1.3 broadcast_in_dim.6.lab_row_ref
  1.3 136.9 %layer.1 = bf16[768,512]{1,0:T(8,128)(2,1)} custom-call(bf16[768,512]{1,0:T(8,128)(2,1)} %q_hbm.1, bf16[768,128]{1,0:T(8,128)(2,1)} %k_ref.1, bf16[768,128]{1,0:T(8,128)(2,1)} %v_ref.1, f32[8]{0:T(128)} %sink_ref.1, s32[1,768]{1,0:T(1,128)} %broadcast_in_dim.6.lab_row_ref, bf16[768,2048]{1,0:T(8,128)(2,1)} %res_hbm.1, bf16[512,2048]{1,0:T(8,128)(2,1)} %wout_hbm.1, ...), custom_call_target="tpu_custom_call" | custom-call | tf_op jit(solution)/shard_map/layer/pallas_call | solution.py:1281
  138.2 2.1 %copy.14 = bf16[768,512]{1,0:T(8,128)(2,1)} copy(bf16[768,512]{1,0:T(8,128)(2,1)} %layer.1) | data formatting | bytes 1572864

commit v4 on v3

--- a/solution.py
+++ b/solution.py
@@ -414,7 +414,7 @@
     q_hbm, k_ref, v_ref, sink_ref, lab_row_ref,
     res_hbm, wout_hbm, gain_ref, wv_hbm, wg_hbm, taps_ref, wd_hbm,
     out_hbm,
-    w3, other, kx, vx, lx, lp, lc, same, part, first, second, mixed, normed, value, gate,
+    w3, other, passing, kx, vx, lx, lp, lc, same, part, first, second, mixed, normed, value, gate,
     pd, box, yin1, zin1, zin2, yin2, res, q_ref, wout_ref, kept, result,
     loc_sem, halo_send, halo_recv, lab_send, lab_recv, zs, zr, xs, xr,
     core_send, core_recv, y_send, y_recv, ag_send, ag_recv, rim_send, rim_recv,
@@ -550,6 +550,18 @@
                 a = spot(s, z, x, width)
                 copy(a, a, xs.at[s, 0], xr.at[s, 0], sibling).start()
 
+    def pass_on(first):
+        for cond, width, rest, _, _ in roles:
+            @pl.when(is_end & cond)
+            def _():
+                b = other.at[2, :, pl.ds(0, rest)]
+                held = passing.at[:, pl.ds(0, rest)]
+                if first:
+                    copy(b, held, xs.at[2, 4], xr.at[2, 4], sibling).start()
+                else:
+                    arrive(held, xr.at[2, 4])
+                    copy(held, spot(2, z, 1 - x, rest), zs.at[2, 4], zr.at[2, 3], beside).start()
+
     owners = (zp, far_mid, far_end)
 
     def event(s, j, who=(0, 1)):
@@ -561,13 +573,16 @@
                     arrive(a, zr.at[s, j])
                     if side == 1 and j == 0:
                         copy(a, a, zs.at[s, 3], zr.at[s, 2], ((3 - z) * 2 + x, tp)).start()
-                    copy(a, a, xs.at[s, j + 1], xr.at[s, j + 1], sibling).start()
+                    if (s, j, side) != (2, 0, 1):
+                        copy(a, a, xs.at[s, j + 1], xr.at[s, j + 1], sibling).start()
 
     def xwait(s, j):
-        for cond, width, _, _, _ in roles:
-            @pl.when(cond)
-            def _():
-                arrive(spot(s, ((z,) + owners)[j], 1 - x, width), xr.at[s, j])
+        for side in range(2):
+            for cond, width, _, _, _ in roles:
+                @pl.when(sides[side] & cond)
+                def _():
+                    where = spot(s, ((z,) + owners)[j], 1 - x, width)
+                    arrive(where, zr.at[2, 3] if (s, j, side) == (2, 1, 1) else xr.at[s, j])
 
     def finish_stream(s):
         for cond, width, rest, _, _ in roles:
@@ -576,7 +591,15 @@
                 left(spot(s, z, x, rest), zs.at[s, 0])
                 left(spot(s, z, x, width), zs.at[s, 1])
                 for j in range(4):
-                    left(spot(s, z, x, width), xs.at[s, j])
+                    if (s, j) != (2, 1):
+                        left(spot(s, z, x, width), xs.at[s, j])
+
+            if s == 2:
+                @pl.when(is_end & cond)
+                def _():
+                    left(spot(s, z, x, width), xs.at[2, 1])
+                    left(spot(s, z, x, rest), xs.at[2, 4])
+                    left(spot(s, z, x, rest), zs.at[2, 4])
 
             @pl.when(is_mid & cond)
             def _():
@@ -606,6 +629,7 @@
     begin_x(1)
     loaded(2)
     begin_x(2, (0,))
+    pass_on(True)
 
     @pl.when(is_narrow)
     def _():
@@ -800,16 +824,17 @@
         share(8 + b, normed_at(pair, core, y, b), (me, partner))
 
     event(1, 0, (0,))
-    far_end_sends(1)
     event(1, 1, (0,))
     serve_spread(0)
+    far_end_sends(1)
     serve_spread(1)
     event(1, 1, (1,))
     begin_end(2)
+    pass_on(False)
     arrive(mixed_at(1 - core, 1 - y), ag_recv.at[2])
     norm(own, part_of(1 - core, 1 - y), piece)
 
-    big = rows // 3
+    big = rows // 2
 
     def project(which, slot):
         def body(t, carry):
@@ -821,7 +846,7 @@
                 gate[slot, r, :] = product
             return carry
 
-        lax.fori_loop(0, 3, body, 0)
+        lax.fori_loop(0, 2, body, 0)
 
     inside = pl.ds(RIM, RIM)
     last = pl.ds(rows, RIM)
@@ -947,13 +972,13 @@
         w = w3[2, pl.ds(pl.multiple_of(t * span, span), span), :]
         for k, slot in enumerate((pair, own)):
             def body(i, carry):
-                r = pl.ds(pl.multiple_of(i * quarter, quarter), quarter)
+                r = pl.ds(pl.multiple_of(i * rows, rows), rows)
                 pd[u, slot, r, :] = lax.dot_general(
                     gate[slot, r, :], w, (((1,), (1,)), ((), ())), preferred_element_type=F32
                 ).astype(BF16)
                 return carry
 
-            lax.fori_loop(0, 2, body, 0)
+            lax.fori_loop(0, 1, body, 0)
 
             @pl.when(core != lax.rem(t, 2))
             def _():
@@ -1238,6 +1263,7 @@
         scratch = [
             pltpu.VMEM((3, n * block, wide), BF16),
             pltpu.VMEM((3, block, wide), BF16),
+            pltpu.VMEM((block, wide), BF16),
             pltpu.VMEM((rows + 2 * WINDOW, kvc), BF16),
             pltpu.VMEM((rows + 2 * WINDOW, kvc), BF16),
             pltpu.VMEM((1, rows + 2 * WINDOW), jnp.int32),
@@ -1265,8 +1291,8 @@
             dma((5, 2)),
             dma((3, 2)), dma((3, 2)),
             dma, dma,
-            dma((3, 4)), dma((3, 3)),
-            dma((3, 4)), dma((3, 4)),
+            dma((3, 5)), dma((3, 4)),
+            dma((3, 5)), dma((3, 5)),
             dma((rows // WINDOW // 2,)), dma((rows // WINDOW // 2,)),
             dma((2,)), dma((2,)),
             dma((12,)), dma((12,)),

time: 141 us -> 137 us (0.972); the launches traced: 140 us -> 135 us
  Pallas kernels: 137 us -> 131 us
    pallas_call x1, Pallas kernels: 137 us -> 131 us  [by_pairs(): pl.pallas_call(functools.partial(paired_kernel, n, ntp), out_shape=jax.Sh...]
where the time goes in v4:
time: 137 us; the launch traced here: 135 us
  Pallas kernels  131 us (96%)
  local copies, waits for them, and re-layouts  3.33 us (2%)
    pallas_call x1, Pallas kernels, by_pairs(): pl.pallas_call(functools.partial(paired_kernel, n, ntp), out_shape=jax.Sh...  131 us

profile of v4, /device:TPU:16, one launch (start us, length us, event | category | flops | bytes accessed | tf_op | source)
XLA Modules:
  0.0 134.8 jit_solution(5372133485199464480)
XLA Ops:
  0.0 1.3 broadcast_in_dim.6.lab_row_ref
  1.3 131.5 %layer.1 = bf16[768,512]{1,0:T(8,128)(2,1)} custom-call(bf16[768,512]{1,0:T(8,128)(2,1)} %q_hbm.1, bf16[768,128]{1,0:T(8,128)(2,1)} %k_ref.1, bf16[768,128]{1,0:T(8,128)(2,1)} %v_ref.1, f32[8]{0:T(128)} %sink_ref.1, s32[1,768]{1,0:T(1,128)} %broadcast_in_dim.6.lab_row_ref, bf16[768,2048]{1,0:T(8,128)(2,1)} %res_hbm.1, bf16[512,2048]{1,0:T(8,128)(2,1)} %wout_hbm.1, ...), custom_call_target="tpu_custom_call" | custom-call | tf_op jit(solution)/shard_map/layer/pallas_call | solution.py:1307
  132.7 2.1 %copy.14 = bf16[768,512]{1,0:T(8,128)(2,1)} copy(bf16[768,512]{1,0:T(8,128)(2,1)} %layer.1) | data formatting | bytes 1572864

commit v5 on v4

--- a/solution.py
+++ b/solution.py
@@ -776,7 +776,7 @@
             normed[slot, r, :] = (m * lax.rsqrt(mean_sq + EPS) * gain_ref[...]).astype(BF16)
             return carry
 
-        lax.fori_loop(0, count // tile, body, 0)
+        lax.fori_loop(0, count // tile, body, 0, unroll=3)
 
     def add_second(i, carry):
         r = pl.ds(pl.multiple_of(i * tile, tile), tile)
@@ -804,8 +804,8 @@
 
     share(0, mixed_at(core, y), (me, across))
     share(1, mixed_at(core, y), (me, partner))
-    norm(own, my_piece, piece)
     for b in range(2):
+        norm(own, my_piece + b * bit, bit)
         share(4 + b, normed_at(own, core, y, b), beside)
     event(0, 0, (0,))
     event(1, 0, (1,))

time: 137 us -> 137 us (level)
  no operation moved by 1% of the time
where the time goes in v5:
time: 137 us; the launch traced here: 135 us
  Pallas kernels  131 us (96%)
  local copies, waits for them, and re-layouts  3.33 us (2%)
    pallas_call x1, Pallas kernels, by_pairs(): pl.pallas_call(functools.partial(paired_kernel, n, ntp), out_shape=jax.Sh...  131 us

profile of v5, /device:TPU:16, one launch (start us, length us, event | category | flops | bytes accessed | tf_op | source)
XLA Modules:
  0.0 134.8 jit_solution(6957115522754497838)
XLA Ops:
  0.0 1.3 broadcast_in_dim.6.lab_row_ref
  1.3 131.5 %layer.1 = bf16[768,512]{1,0:T(8,128)(2,1)} custom-call(bf16[768,512]{1,0:T(8,128)(2,1)} %q_hbm.1, bf16[768,128]{1,0:T(8,128)(2,1)} %k_ref.1, bf16[768,128]{1,0:T(8,128)(2,1)} %v_ref.1, f32[8]{0:T(128)} %sink_ref.1, s32[1,768]{1,0:T(1,128)} %broadcast_in_dim.6.lab_row_ref, bf16[768,2048]{1,0:T(8,128)(2,1)} %res_hbm.1, bf16[512,2048]{1,0:T(8,128)(2,1)} %wout_hbm.1, ...), custom_call_target="tpu_custom_call" | custom-call | tf_op jit(solution)/shard_map/layer/pallas_call | solution.py:1307
  132.7 2.1 %copy.14 = bf16[768,512]{1,0:T(8,128)(2,1)} copy(bf16[768,512]{1,0:T(8,128)(2,1)} %layer.1) | data formatting | bytes 1572864
